TPU v7x, 512 devices: a whole 4x8x8 slice. The times are simulated.
512 devices in a mesh: sp: 64 (over z, y), tp: 8 (over x, core).
Axes of the slice: x: 4, y: 8, z: 8, core: 2. Of those that a mesh axis runs over, the one named last changes fastest.
Arguments:
- tokens: bfloat16 [8192, 4096], P('sp'), may hold values from -6 to 6
- norm_gain: float32 [4096], replicated, may hold values from 0.1 to 1.9
- w_query: bfloat16 [4096, 2048], P('sp', 'tp'), may hold values from -1 to 1
- w_key: bfloat16 [4096, 512], P('sp', 'tp'), may hold values from -1 to 1
- w_value: bfloat16 [4096, 512], P('sp', 'tp'), may hold values from -0.09375 to 0.09375
- w_state_in: bfloat16 [4096, 2048], P('sp', 'tp'), may hold values from -0.09375 to 0.09375
- sink_logit: float32 [32], P('tp'), may hold values from 2 to 6
- decay_rate: float32 [128, 64], P('tp'), may hold values from 0.0002 to 4
- rotation: float32 [128, 64], P('tp'), may hold values from 1 to 60
- log_step: float32 [128], P('tp'), may hold values from -5.3 to -3
- in_re: float32 [128, 64, 16], P('tp'), may hold values from -1.5 to 1.5
- in_im: float32 [128, 64, 16], P('tp'), may hold values from -1.5 to 1.5
- out_re: float32 [128, 16, 64], P('tp'), may hold values from -0.75 to 0.75
- out_im: float32 [128, 16, 64], P('tp'), may hold values from -0.75 to 0.75
- skip_gain: float32 [2048], P('tp'), may hold values from -4 to 4
- w_attn_out: bfloat16 [2048, 4096], P('tp', 'sp'), may hold values from -0.5 to 0.5
- w_state_out: bfloat16 [2048, 4096], P('tp', 'sp'), may hold values from -0.125 to 0.125
- out_gain: float32 [4096], replicated, may hold values from 0.1 to 1.9
Outputs:
- mixed: bfloat16 [8192, 4096], P(('sp', 'tp'))
All inputs are finite; a program needn't handle non-finite values.
Results may differ from a plain program's by a relative error of at most 0.015.
The roundings to bfloat16 on the way count: a program that leaves them out, or rounds other values in their place, can miss the bound.
Values may be sent and summed in bfloat16 or wider, within the bound.
A program may use at most 64 MiB of HBM per device.

v0:
```python
import math

import jax
import jax.numpy as jnp
from jax import lax
from jax.sharding import PartitionSpec as P

HEAD = 64
WINDOW = 128


epsilon = 1e-06
rotary_base = 500000.0


def copy_for_each(value, axis):
    size = lax.axis_size(axis)
    return lax.all_to_all(
        jnp.broadcast_to(value[None], (size, *value.shape)), axis, 0, 0, tiled=True
    )


def gathered_once(value, axis):
    leaves = jax.tree.leaves(value)
    sequence = sorted(range(len(leaves)), key=lambda k: -leaves[k].size)
    width = (1, *leaves[sequence[0]].shape)[-1]
    lines = [
        jnp.pad(leaves[k].reshape(-1), (0, -leaves[k].size % width)).reshape(-1, width)
        for k in sequence
    ]
    both, at, found = (copy_for_each(jnp.concatenate(lines), axis), 0, {})
    for k, line in zip(sequence, lines):
        section = both[:, at : at + len(line)].reshape(len(both), -1)
        found[k] = section[:, : leaves[k].size].reshape(-1, *leaves[k].shape)
        at += len(line)
    numbers = iter(range(len(leaves)))
    return jax.tree.map(lambda _: found[next(numbers)], value)


def combined_pairwise(pieces, combine):
    while len(jax.tree.leaves(pieces)[0]) > 1:
        pieces = jax.vmap(combine)(
            *(jax.tree.map(lambda part: part[side::2], pieces) for side in (0, 1))
        )
    return jax.tree.map(lambda part: part[0], pieces)


def entering(value, axis, combine, identity):
    size, mine = (lax.axis_size(axis), lax.axis_index(axis))
    passed = jnp.arange(size) < mine

    def kept(part, zero, own):
        part = jnp.where(
            passed.reshape(-1, *(1 for _ in own.shape)), part, jnp.asarray(zero, own.dtype)
        )
        return part

    pieces = gathered_once(value, axis)
    return combined_pairwise(jax.tree.map(kept, pieces, identity, value), combine)


def passed_along(value, axis, by):
    size = lax.axis_size(axis)
    pairs = [(i, i + by) for i in range(size) if 0 <= i + by < size]
    return lax.ppermute(value, axis, pairs)


def side_by_side(arrays, axis, dim, along):
    ends, at = ([], 0)
    for a in arrays[:-1]:
        at += a.shape[along]
        ends.append(at)
    both = jnp.concatenate(arrays, axis=along)
    return tuple(jnp.split(lax.all_gather(both, axis, axis=dim, tiled=True), ends, axis=along))


def gather_turned(arrays, axis, dims):
    turned = [jnp.moveaxis(a, dim, 0) for a, dim in zip(arrays, dims)]
    widths = [t[0].size for t in turned]
    both = jnp.concatenate([t.reshape(-1, w) for t, w in zip(turned, widths)], axis=1)
    out = lax.all_gather(both, axis, axis=0, tiled=True)
    blocks = jnp.split(out, [sum(widths[:k]) for k in range(1, len(widths))], axis=1)
    return tuple(
        (
            jnp.moveaxis(b.reshape(-1, *t.shape[1:]), 0, dim)
            for b, t, dim in zip(blocks, turned, dims)
        )
    )


def cut_along(value, dim, size):
    dims = value.shape
    blocks = value.reshape(*dims[:dim], size, dims[dim] // size, *dims[dim + 1 :])
    return jnp.moveaxis(blocks, dim, 0)


def sum_at_owner(value, axis, dim):
    blocks = cut_along(value, dim, lax.axis_size(axis))
    arrived = lax.all_to_all(blocks, axis, split_axis=0, concat_axis=0, tiled=True)
    return arrived.astype(jnp.float32).sum(axis=0)


def rotate(heads_block, positions):
    head_width = heads_block.shape[-1]
    half_width = head_width // 2
    frequency = rotary_base ** (-(jnp.arange(half_width, dtype=jnp.float32) * 2.0 / head_width))
    angles = positions.astype(jnp.float32)[:, None] * frequency[None, :]
    cosine = jnp.cos(angles)[:, None, :]
    sine_part = jnp.sin(angles)[:, None, :]
    lower_half = heads_block[..., :half_width]
    upper_half = heads_block[..., half_width:]
    return jnp.concatenate(
        [
            lower_half * cosine - upper_half * sine_part,
            upper_half * cosine + lower_half * sine_part,
        ],
        axis=-1,
    )


def shape_heads(query_sum, key_sum, value_sum, positions, head_width):
    row_count = query_sum.shape[0]
    kv_heads = key_sum.shape[1] // head_width
    group_size = query_sum.shape[1] // key_sum.shape[1]
    queries = rotate(
        query_sum.reshape(row_count, kv_heads * group_size, head_width), positions
    ).astype(jnp.bfloat16)
    queries = queries.reshape(row_count, kv_heads, group_size, head_width)
    key_rows = rotate(key_sum.reshape(row_count, kv_heads, head_width), positions).astype(
        jnp.bfloat16
    )
    key_rows = key_rows.reshape(row_count, kv_heads * head_width)
    value_rows = value_sum.astype(jnp.bfloat16)
    return (queries, key_rows, value_rows)


def band_attention(queries, key_rows, value_rows, sink_logit, first_row, window):
    row_count, kv_heads, group_size, head_width = queries.shape
    blocks = row_count // window
    query_blocks = queries.reshape(blocks, window, kv_heads, group_size, head_width)
    key_blocks = jnp.concatenate(
        [
            key_rows[:row_count].reshape(blocks, window, kv_heads, head_width),
            key_rows[window:].reshape(blocks, window, kv_heads, head_width),
        ],
        axis=1,
    )
    value_blocks = jnp.concatenate(
        [
            value_rows[:row_count].reshape(blocks, window, kv_heads, head_width),
            value_rows[window:].reshape(blocks, window, kv_heads, head_width),
        ],
        axis=1,
    )
    scores = jnp.einsum(
        "bqkgd,bskd->bkgqs", query_blocks, key_blocks, preferred_element_type=jnp.float32
    ) / math.sqrt(head_width)
    block_start = jnp.arange(blocks, dtype=jnp.int32)[:, None, None] * window
    query_at = first_row + block_start + jnp.arange(window, dtype=jnp.int32)[None, :, None]
    key_at = (
        first_row - window + block_start + jnp.arange(2 * window, dtype=jnp.int32)[None, None, :]
    )
    offset_gap = query_at - key_at
    visible = (offset_gap >= 0) & (offset_gap < window) & (key_at >= 0)
    scores = jnp.where(visible[:, None, None, :, :], scores, -jnp.inf)
    sink_value = sink_logit.reshape(1, kv_heads, group_size, 1, 1)
    top_score = jnp.maximum(jnp.max(scores, axis=-1, keepdims=True), sink_value)
    exponent = jnp.exp(scores - top_score)
    totals = jnp.sum(exponent, axis=-1, keepdims=True) + jnp.exp(sink_value - top_score)
    weights = (exponent / totals).astype(jnp.bfloat16)
    attended = jnp.einsum(
        "bkgqs,bskd->bqkgd", weights, value_blocks, preferred_element_type=jnp.float32
    )
    return attended.reshape(row_count, kv_heads * group_size * head_width).astype(jnp.bfloat16)


def discretize(decay_rate, rotation, log_step, in_re, in_im):
    time_step = jnp.exp(log_step)[:, None]
    lambda_re = -decay_rate
    modulus = jnp.exp(lambda_re * time_step)
    pole_re = modulus * jnp.cos(rotation * time_step)
    pole_im = modulus * jnp.sin(rotation * time_step)
    minus_one = pole_re - 1.0
    denominator = lambda_re * lambda_re + rotation * rotation
    factor_re = ((minus_one * lambda_re + pole_im * rotation) / denominator)[..., None]
    factor_im = ((pole_im * lambda_re - minus_one * rotation) / denominator)[..., None]
    drive_re = factor_re * in_re - factor_im * in_im
    drive_im = factor_re * in_im + factor_im * in_re
    return (pole_re, pole_im, drive_re, drive_im)


def chain_link(earlier, later):
    early_are, early_aim, early_bre, early_bim = earlier
    late_are, late_aim, late_bre, late_bim = later
    return (
        late_are * early_are - late_aim * early_aim,
        late_are * early_aim + late_aim * early_are,
        late_are * early_bre - late_aim * early_bim + late_bre,
        late_are * early_bim + late_aim * early_bre + late_bim,
    )


def local_states(inputs, pole_re, pole_im, drive_re, drive_im):
    row_count = inputs.shape[0]
    groups, states, group_width = drive_re.shape
    channel_values = inputs.astype(jnp.float32).reshape(row_count, groups, group_width)
    push_re = jnp.einsum("tgh,gph->tgp", channel_values, drive_re).reshape(
        row_count, groups * states
    )
    push_im = jnp.einsum("tgh,gph->tgp", channel_values, drive_im).reshape(
        row_count, groups * states
    )
    decay_re = jnp.broadcast_to(pole_re.reshape(1, groups * states), push_re.shape)
    decay_im = jnp.broadcast_to(pole_im.reshape(1, groups * states), push_im.shape)
    return lax.associative_scan(chain_link, (decay_re, decay_im, push_re, push_im), axis=0)


def apply_carry(running, carry_re, carry_im):
    power_re, power_im, own_re, own_im = running
    return (
        own_re + power_re * carry_re - power_im * carry_im,
        own_im + power_re * carry_im + power_im * carry_re,
    )


def read_out(inputs, state_re, state_im, out_re, out_im, skip_gain):
    row_count = inputs.shape[0]
    groups, group_width, states = out_re.shape
    grid_re = state_re.reshape(row_count, groups, states)
    grid_im = state_im.reshape(row_count, groups, states)
    summed = jnp.einsum("tgp,ghp->tgh", grid_re, out_re) - jnp.einsum(
        "tgp,ghp->tgh", grid_im, out_im
    )
    summed = summed.reshape(row_count, groups * group_width) + skip_gain * inputs.astype(
        jnp.float32
    )
    return jax.nn.gelu(summed).astype(jnp.bfloat16)


def chain_in(power_re, power_im, end_re, end_im):
    identity = (
        jnp.ones_like(power_re),
        jnp.zeros_like(power_im),
        jnp.zeros_like(end_re),
        jnp.zeros_like(end_im),
    )
    before = entering((power_re, power_im, end_re, end_im), "sp", chain_link, identity)
    return (before[2], before[3])


def state_branch(inputs, decay_rate, rotation, log_step, in_re, in_im, out_re, out_im, skip_gain):
    pole_re, pole_im, drive_re, drive_im = discretize(decay_rate, rotation, log_step, in_re, in_im)
    running = local_states(inputs, pole_re, pole_im, drive_re, drive_im)
    carry_re, carry_im = chain_in(running[0][-1], running[1][-1], running[2][-1], running[3][-1])
    state_re, state_im = apply_carry(running, carry_re, carry_im)
    return read_out(inputs, state_re, state_im, out_re, out_im, skip_gain)


def earlier_window(key_rows, value_rows):
    joined = jnp.concatenate([key_rows, value_rows], axis=1)
    prior = passed_along(joined, "sp", 1)
    return jnp.concatenate([prior, joined], axis=0)


def make_adder(normed_cols):

    def add_pieces(carried, weight_pieces, row_start):
        updated = []
        for running_total, weight_piece in zip(carried, weight_pieces):
            product = lax.dot_general(
                normed_cols,
                weight_piece,
                (((0,), (0,)), ((), ())),
                preferred_element_type=jnp.float32,
            )
            updated.append(product)
        return tuple(updated)

    return add_pieces


def body(
    tokens,
    norm_gain,
    w_query,
    w_key,
    w_value,
    w_state_in,
    sink_logit,
    decay_rate,
    rotation,
    log_step,
    in_re,
    in_im,
    out_re,
    out_im,
    skip_gain,
    w_attn_out,
    w_state_out,
    out_gain,
):
    row_count = tokens.shape[0]
    window = WINDOW
    head_width = HEAD
    wide_tokens = tokens.astype(jnp.float32)
    normed = (
        wide_tokens
        * lax.rsqrt(jnp.mean(wide_tokens * wide_tokens, axis=-1, keepdims=True) + epsilon)
        * norm_gain
    ).astype(jnp.bfloat16)
    first_row = lax.axis_index("sp") * row_count
    positions = first_row + jnp.arange(row_count, dtype=jnp.int32)
    add_pieces = make_adder(jnp.transpose(normed))

    def empty_like(weight_shard):
        return jnp.zeros((row_count, weight_shard.shape[1]), jnp.float32)

    query_sum, key_sum, value_sum, input_sum = add_pieces(
        (empty_like(w_query), empty_like(w_key), empty_like(w_value), empty_like(w_state_in)),
        side_by_side((w_query, w_key, w_value, w_state_in), "sp", 0, 1),
        jnp.int32(0),
    )
    queries, key_rows, value_rows = shape_heads(
        query_sum, key_sum, value_sum, positions, head_width
    )
    joined_rows = earlier_window(key_rows, value_rows)
    inputs = input_sum.astype(jnp.bfloat16)
    mixed_state = state_branch(
        inputs, decay_rate, rotation, log_step, in_re, in_im, out_re, out_im, skip_gain
    )
    kv_width = key_rows.shape[1]
    kv_heads = kv_width // head_width
    all_keys = joined_rows[:, :kv_width].reshape(window + row_count, kv_heads, head_width)
    all_values = joined_rows[:, kv_width:].reshape(window + row_count, kv_heads, head_width)
    attended = band_attention(queries, all_keys, all_values, sink_logit, first_row, window)
    attn_rows, state_rows = gather_turned((w_attn_out, w_state_out), "sp", (1, 1))
    projected = sum_at_owner(
        (
            jnp.dot(attended, attn_rows, preferred_element_type=jnp.float32)
            + jnp.dot(mixed_state, state_rows, preferred_element_type=jnp.float32)
        ).astype(jnp.bfloat16),
        "tp",
        0,
    )
    row_scale = lax.rsqrt(jnp.mean(projected * projected, axis=-1, keepdims=True) + epsilon)
    return (projected * row_scale * out_gain).astype(jnp.bfloat16)


def solution(mesh):
    return jax.shard_map(
        body,
        mesh=mesh,
        in_specs=(
            P("sp", None),
            P(),
            P("sp", "tp"),
            P("sp", "tp"),
            P("sp", "tp"),
            P("sp", "tp"),
            P("tp"),
            P("tp", None),
            P("tp", None),
            P("tp"),
            P("tp", None, None),
            P("tp", None, None),
            P("tp", None, None),
            P("tp", None, None),
            P("tp"),
            P("tp", "sp"),
            P("tp", "sp"),
            P(),
        ),
        out_specs=P(("sp", "tp"), None),
        check_vma=False,
    )
```

profile of v0, /device:TPU:1, one launch (start us, length us, event | category | flops | bytes accessed | tf_op | source)
XLA Modules:
  0.0 313.3 jit_solution(12318455763996068841)
XLA Ops:
  6.5 1.6 pad_maximum_fusion.8
  18.4 81.6 %all-gather.3.cloned.1.call-done = bf16[4096,640]{1,0:T(8,128)(2,1)} async-done(((bf16[64,640]{1,0:T(8,128)(2,1)}), bf16[4096,640]{1,0:T(8,128)(2,1)}) %all-gather.3.cloned.1.call-update) | async-done | bytes 5242896 | tf_op jit(solution)/shard_map/all_gather | solution.py:74
  100.0 2.4 fusion.13
  103.6 11.3 %slice.561 = f32[64,1024]{0,1:T(8,128)} slice(f32[128,1024]{0,1:T(8,128)S(1)} %bitcast.76), slice={[1:128:2], [0:1024:1]} | slice | bytes 524288 | tf_op jit(solution)/shard_map/slice | solution.py:215
  114.9 10.1 %slice.558 = f32[64,1024]{0,1:T(8,128)S(1)} slice(f32[128,1024]{0,1:T(8,128)S(1)} %bitcast.77), slice={[0:127:2], [0:1024:1]} | slice | bytes 524288 | tf_op jit(solution)/shard_map/slice | solution.py:215
  125.0 10.7 %slice.638 = f32[63,1024]{0,1:T(8,128)S(1)} slice(f32[128,1024]{0,1:T(8,128)S(1)} %bitcast.78), slice={[2:128:2], [0:1024:1]} | slice | bytes 516096 | tf_op jit(solution)/shard_map/slice | solution.py:215
  135.7 11.3 %slice.567 = f32[64,1024]{0,1:T(8,128)} slice(f32[128,1024]{0,1:T(8,128)S(1)} %bitcast.80), slice={[1:128:2], [0:1024:1]} | slice | bytes 524288 | tf_op jit(solution)/shard_map/slice | solution.py:215
  147.0 10.1 %slice.560 = f32[64,1024]{0,1:T(8,128)S(1)} slice(f32[128,1024]{0,1:T(8,128)S(1)} %bitcast.81), slice={[0:127:2], [0:1024:1]} | slice | bytes 524288 | tf_op jit(solution)/shard_map/slice | solution.py:215
  157.1 10.9 %slice.656 = f32[63,1024]{0,1:T(8,128)S(1)} slice(f32[128,1024]{0,1:T(8,128)S(1)} %bitcast.82), slice={[2:128:2], [0:1024:1]} | slice | bytes 516096 | tf_op jit(solution)/shard_map/slice | solution.py:215
  192.7 1.9 convolution_bitcast_fusion
  194.8 2.3 convolution_convert_fusion.1
  197.9 3.5 %collective-permute-start = (bf16[128,128]{0,1:T(8,128)(2,1)}, bf16[128,128]{0,1:T(8,128)(2,1)}, u32[]{:S(2)}, u32[]{:S(2)}) collective-permute-start(bf16[128,128]{0,1:T(8,128)(2,1)} %pad_maximum_fusion.14), channel_id=1, source_target_pairs={{0,8},{8,16},{16,24},{24,32},{32,40},{40,48},{48,56},{56,64},{64,7... | collective-permute-start | bytes 98312 | tf_op jit(solution)/shard_map/ppermute | solution.py:65
  213.7 2.7 pad.225
  216.4 1.7 pad.227
  221.0 8.3 %all-to-all-start = ((f32[64,4,1024]{2,1,0:T(4,128)}), f32[64,4,1024]{2,1,0:T(4,128)S(1)}, u32[]{:S(2)}, u32[]{:S(2)}) async-start(f32[64,4,1024]{2,1,0:T(4,128)} %broadcast_in_dim.87), calls=%async_computation | async-start | bytes 2097152 | tf_op jit(solution)/shard_map/all_to_all | solution.py:18
  229.4 2.6 fusion.9
  233.7 2.4 fusion.7
  236.1 17.2 %all-to-all-done = f32[64,4,1024]{2,1,0:T(4,128)S(1)} async-done(((f32[64,4,1024]{2,1,0:T(4,128)}), f32[64,4,1024]{2,1,0:T(4,128)S(1)}, u32[]{:S(2)}, u32[]{:S(2)}) %all-to-all-start) | async-done | bytes 1048608 | tf_op jit(solution)/shard_map/all_to_all | solution.py:18
  256.1 1.7 multiply_subtract_fusion.2
  257.8 1.6 slice.665
  262.5 1.5 slice.666
  271.6 3.0 multiply_add_fusion
  277.4 2.4 fusion
  279.8 25.6 %all_to_all.10 = bf16[8,16,4096]{2,1,0:T(8,128)(2,1)S(1)} all-to-all(bf16[8,16,4096]{2,1,0:T(8,128)(2,1)S(1)} %bitcast.84), channel_id=1, replica_groups=mesh['sp'=64,'tp'=8] {'tp'}, dimensions={0} | all-to-all | bytes 2097152 | tf_op jit(solution)/shard_map/all_to_all | solution.py:99
  (462 shorter events, 69.1 us)
Async XLA Ops:
  6.5 269.5 %copy-start = (f32[16,16,64]{2,1,0:T(8,128)S(1)}, f32[16,16,64]{2,1,0:T(8,128)}, u32[]{:S(2)}) copy-start(f32[16,16,64]{2,1,0:T(8,128)} %param.30) | copy-start | bytes 196612
  6.5 93.5 %all-gather.3.cloned.1.call-start = ((), (), s32[]{:S(2)}) async-start(), calls=%async_computation.2 | async-start | bytes 5324800 | tf_op jit(solution)/shard_map/all_gather | solution.py:74
  8.1 225.5 %all-gather.5.cloned.1.call-start = ((), (), s32[]{:S(2)}) async-start(), calls=%async_computation.3 | async-start | bytes 4259840 | tf_op jit(solution)/shard_map/all_gather | solution.py:81
  13.6 88.8 %copy-start.100 = (f32[128]{0:T(128)}, f32[128]{0:T(128)S(1)}, u32[]{:S(2)}) copy-start(f32[128]{0:T(128)S(1)} %add_rsqrt_fusion.1) | copy-start | bytes 1540
  18.4 84.7 %copy-start.12 = (f32[16,64,16]{1,2,0:T(8,128)S(1)}, f32[16,64,16]{1,2,0:T(8,128)}, u32[]{:S(2)}) copy-start(f32[16,64,16]{1,2,0:T(8,128)} %param.28) | copy-start | bytes 196612
  18.4 84.7 %copy-start.13 = (f32[16,64,16]{1,2,0:T(8,128)S(1)}, f32[16,64,16]{1,2,0:T(8,128)}, u32[]{:S(2)}) copy-start(f32[16,64,16]{1,2,0:T(8,128)} %param.29) | copy-start | bytes 196612
  175.3 17.4 %copy-start.9 = (bf16[128,4096]{1,0:T(8,128)(2,1)S(1)}, bf16[128,4096]{1,0:T(8,128)(2,1)}, u32[]{:S(2)}) copy-start(bf16[128,4096]{1,0:T(8,128)(2,1)} %param.18) | copy-start | bytes 3145732
  183.7 10.8 %copy-start.92 = (f32[128]{0:T(128)S(1)}, f32[128]{0:T(128)}, u32[]{:S(2)}) copy-start(f32[128]{0:T(128)} %copy-done.91) | copy-start | bytes 1540
  183.8 10.8 %copy-start.94 = (f32[32]{0:T(128)S(1)}, f32[32]{0:T(128)}, u32[]{:S(2)}) copy-start(f32[32]{0:T(128)} %copy-done.93) | copy-start | bytes 388
  183.8 11.0 %copy-start.98 = (f32[4096]{0:T(1024)S(1)}, f32[4096]{0:T(1024)}, u32[]{:S(2)}) copy-start(f32[4096]{0:T(1024)} %param.19) | copy-start | bytes 49156
  183.8 11.0 %copy-start.101 = (f32[128]{0:T(128)S(1)}, f32[128]{0:T(128)}, u32[]{:S(2)}) copy-start(f32[128]{0:T(128)} %copy-done.100) | copy-start | bytes 1540
  197.9 34.2 %collective-permute-start = (bf16[128,128]{0,1:T(8,128)(2,1)}, bf16[128,128]{0,1:T(8,128)(2,1)}, u32[]{:S(2)}, u32[]{:S(2)}) collective-permute-start(bf16[128,128]{0,1:T(8,128)(2,1)} %pad_maximum_fusion.14), channel_id=1, source_target_pairs={{0,8},{8,16},{16,24},{24,32},{32,40},{40,48},{48,56},{56,64},{64,7... | collective-permute-start | bytes 98312 | tf_op jit(solution)/shard_map/ppermute | solution.py:65
  208.5 9.6 %copy-start.1 = (f32[128,1024]{1,0:T(8,128)}, f32[128,1024]{1,0:T(8,128)S(1)}, u32[]{:S(2)}) copy-start(f32[128,1024]{1,0:T(8,128)S(1)} %pad.198) | copy-start | bytes 1572868
  209.7 8.4 %copy-start.3 = (f32[128,1024]{1,0:T(8,128)}, f32[128,1024]{1,0:T(8,128)S(1)}, u32[]{:S(2)}) copy-start(f32[128,1024]{1,0:T(8,128)S(1)} %pad.228) | copy-start | bytes 1572868
  209.8 8.3 %copy-start.5 = (f32[128,1024]{1,0:T(8,128)}, f32[128,1024]{1,0:T(8,128)S(1)}, u32[]{:S(2)}) copy-start(f32[128,1024]{1,0:T(8,128)S(1)} %pad.199) | copy-start | bytes 1572868
  211.8 9.2 %copy-start.7 = (f32[128,1024]{1,0:T(8,128)}, f32[128,1024]{1,0:T(8,128)S(1)}, u32[]{:S(2)}) copy-start(f32[128,1024]{1,0:T(8,128)S(1)} %pad.226) | copy-start | bytes 1572868
  216.4 12.9 %copy-start.99 = (f32[4096]{0:T(1024)S(1)}, f32[4096]{0:T(1024)}, u32[]{:S(2)}) copy-start(f32[4096]{0:T(1024)} %param.19) | copy-start | bytes 49156
  218.1 11.2 %copy-start.102 = (f32[128]{0:T(128)S(1)}, f32[128]{0:T(128)}, u32[]{:S(2)}) copy-start(f32[128]{0:T(128)} %copy-done.100) | copy-start | bytes 1540
  218.2 11.2 %copy-start.10 = (bf16[128,4096]{1,0:T(8,128)(2,1)S(1)}, bf16[128,4096]{1,0:T(8,128)(2,1)}, u32[]{:S(2)}) copy-start(bf16[128,4096]{1,0:T(8,128)(2,1)} %param.18) | copy-start | bytes 3145732
  221.0 32.3 %all-to-all-start = ((f32[64,4,1024]{2,1,0:T(4,128)}), f32[64,4,1024]{2,1,0:T(4,128)S(1)}, u32[]{:S(2)}, u32[]{:S(2)}) async-start(f32[64,4,1024]{2,1,0:T(4,128)} %broadcast_in_dim.87), calls=%async_computation | async-start | bytes 2097152 | tf_op jit(solution)/shard_map/all_to_all | solution.py:18
  236.1 18.0 %copy-start.97 = (pred[64]{0:T(512)(128)(4,1)S(1)}, pred[64]{0:T(512)(128)(4,1)}, u32[]{:S(2)}) copy-start(pred[64]{0:T(512)(128)(4,1)} %iota_compare_fusion) | copy-start | bytes 196
  257.8 13.8 %copy-start.2 = (f32[128,1024]{1,0:T(8,128)S(1)}, f32[128,1024]{1,0:T(8,128)}, u32[]{:S(2)}) copy-start(f32[128,1024]{1,0:T(8,128)} %copy-done.1) | copy-start | bytes 1572868
  257.8 13.8 %copy-start.4 = (f32[128,1024]{1,0:T(8,128)S(1)}, f32[128,1024]{1,0:T(8,128)}, u32[]{:S(2)}) copy-start(f32[128,1024]{1,0:T(8,128)} %copy-done.3) | copy-start | bytes 1572868
  279.8 25.9 %copy-start.75 = (f32[4096]{0:T(1024)S(1)}, f32[4096]{0:T(1024)}, u32[]{:S(2)}) copy-start(f32[4096]{0:T(1024)} %param.35) | copy-start | bytes 49156
  (83 other events, 344.9 us)
Sparse Core Ops, SparseCore 0:
  10.3 89.6 all-gather.2
  103.1 82.9 all-gather.4
where the time goes:
time: 315 us; the launch traced here: 313 us
  local copies, waits for them, and re-layouts  116 us (37%)
  waiting for transfers between devices  98.9 us (31%)
  other arithmetic  29 us (9%)
  blocking collectives  25.6 us (8%)
  matrix products  16.3 us (5%)
  between operations  15.7 us (5%)
  starting transfers between devices  11.9 us (4%)
    slice x47, local copies, waits for them, and re-layouts, local_states(): lax.associative_scan(chain_link, (decay_re, decay_im, push_re, push_im),...  82.6 us
    all_gather x1, waiting for transfers between devices, side_by_side(): lax.all_gather(both, axis, axis=dim, tiled=True)  81.6 us
    all_to_all x1, blocking collectives, sum_at_owner(): lax.all_to_all(blocks, axis, split_axis=0, concat_axis=0, tiled=True)  25.6 us
    all_to_all x1, waiting for transfers between devices, copy_for_each(): lax.all_to_all(jnp.broadcast_to(value[None], (size, *value.shape)), axis,...  17.2 us
    slice x40, local copies, waits for them, and re-layouts, combined_pairwise(): part[side::2]  13.3 us
    dot_general x4, matrix products, add_pieces(): lax.dot_general(normed_cols, weight_piece, (((0,), (0,)), ((), ())), pref...  9.16 us
    pad x48, local copies, waits for them, and re-layouts, local_states(): lax.associative_scan(chain_link, (decay_re, decay_im, push_re, push_im),...  8.91 us
    all_to_all x1, starting transfers between devices, copy_for_each(): lax.all_to_all(jnp.broadcast_to(value[None], (size, *value.shape)), axis,...  8.29 us
  transfers between devices with their start and end apart: 4, of which 2 were waited for; matrix products, arithmetic and copies ran while one was open for 42% of the time, Pallas kernels for 0%

commit v1 on v0

v1 whole, which is shorter than its diff:
```python
import math

import jax
import jax.numpy as jnp
from jax import lax
from jax.experimental import pallas as pl
from jax.experimental.pallas import tpu as pltpu
from jax.sharding import PartitionSpec as P

MESH = pl.DeviceIdType.MESH
F32 = jnp.float32
BF16 = jnp.bfloat16
EPS = 1e-06
BASE = 500000.0
RING = 8
TP = 8
ROWS = 128
D = 4096
NIN = 640
NST = 1024
FLOWS = tuple((half, side) for half in (0, 1) for side in (0, 1))


def nn(a, b):
    return lax.dot_general(a, b, (((1,), (0,)), ((), ())), preferred_element_type=F32)


def nt(a, b):
    return lax.dot_general(a, b, (((1,), (1,)), ((), ())), preferred_element_type=F32)


def split(x):
    high = x.astype(BF16)
    return high, (x - high.astype(F32)).astype(BF16)


def iota(shape, dim):
    return lax.broadcasted_iota(jnp.int32, shape, dim)


def ring(v, d):
    return lax.rem(v + d + 2 * RING, RING)


def cmul(ar, ai, br, bi):
    return ar * br - ai * bi, ar * bi + ai * br


def kernel(
    tok_h, ng_h, wq_h, wk_h, wv_h, ws_h, sink_s, dec_h, rot_h, ls_s,
    inre_h, inim_h, outre_h, outim_h, sg_h, wa_h, wso_h, og_h,
    out_ref,
    W, Wo, tok, xn, kw, vw, ng, og, sg, dec, rot, inre, inim, outre, outim,
    qkvs, cosr, sinr, prow, pw, BDi, BDo, Sr, Si, Er, Ei, Cr, Ci, CY, CZ, KVb, qb, M, Pb, R,
    lsem, w_ssem, w_r1, w_r2, o_ssem, o_r1, o_r2, kv_ss, kv_rs, cy_ss, cy_rs, cz_ss, cz_rs,
    rs_ss, rs_rs,
):
    sp = lax.axis_index("sp")
    t = lax.axis_index("tp")
    z = sp // RING
    y = lax.rem(sp, RING)

    local = [
        (wq_h, W.at[sp, :, pl.ds(0, 256)]),
        (ws_h, W.at[sp, :, pl.ds(256, 256)]),
        (wk_h, kw),
        (wv_h, vw),
        (tok_h, tok),
        (ng_h, ng),
        (dec_h, dec),
        (rot_h, rot),
        (inre_h, inre),
        (inim_h, inim),
        (outre_h, outre),
        (outim_h, outim),
        (wa_h, Wo.at[sp, :, pl.ds(0, 256)]),
        (wso_h, Wo.at[sp, :, pl.ds(256, 256)]),
        (sg_h, sg),
        (og_h, og),
    ]
    copies = [pltpu.make_async_copy(a, b, lsem.at[i]) for i, (a, b) in enumerate(local)]
    for c in copies:
        c.start()

    barrier = pltpu.get_barrier_semaphore()
    after = lax.rem(sp + 1, RING * RING)
    before = lax.rem(sp + RING * RING - 1, RING * RING)
    peers = [(z * RING + ring(y, j), t) for j in range(1, RING)]
    peers += [(ring(z, j) * RING + y, t) for j in range(1, RING)]
    peers += [(sp, lax.rem(t + j, TP)) for j in range(1, TP)]
    peers += [(after, t), (before, t)]
    for peer in peers:
        pl.semaphore_signal(barrier, inc=1, device_id=peer, device_id_type=MESH)

    for i in range(4):
        copies[i].wait()
    lane64 = iota((64, 128), 1)
    row64 = iota((64, 128), 0)
    to_low = (lane64 == row64).astype(F32).astype(BF16)
    to_high = (lane64 == row64 + 64).astype(F32).astype(BF16)
    W[sp, :, 512:640] = (nn(kw[...], to_low) + nn(vw[...], to_high)).astype(BF16)
    pl.semaphore_wait(barrier, len(peers))

    def block(half, d1, d2):
        if half == 0:
            return ring(z, d1) * RING + ring(y, d2)
        return ring(z, d2) * RING + ring(y, d1)

    def neighbour(half, phase, side):
        step = 1 if side == 0 else -1
        if (half == 0) == (phase == 1):
            return (ring(z, step) * RING + y, t)
        return (z * RING + ring(y, step), t)

    def rows(half, hop, side):
        if hop < 4:
            return pl.ds(32 * half, 32)
        return pl.ds(32 * half + 16 * side, 16)

    def piece(buf, ssem, rsem, half, phase, hop, side, index):
        ref = buf.at[index, rows(half, hop, side)]
        return pltpu.make_async_remote_copy(
            src_ref=ref, dst_ref=ref, send_sem=ssem, recv_sem=rsem,
            device_id=neighbour(half, phase, side), device_id_type=MESH,
        )

    def sign(side):
        return 1 if side == 0 else -1

    def offset(k):
        if isinstance(k, int):
            return k // 2 if k % 2 == 0 else -((k + 1) // 2)
        return (1 - 2 * lax.rem(k, 2)) * ((k + 1) // 2)

    class Gather:
        def __init__(self, buf, ssem, r1, r2):
            self.buf, self.ssem, self.r1, self.r2 = buf, ssem, r1, r2

        def first(self, half, side, hop, back):
            index = block(half, -(hop - 1 + back) * sign(side), 0)
            return piece(self.buf, self.ssem, self.r1.at[half, side, hop - 1],
                         half, 1, hop, side, index)

        def second(self, half, side, hop, k, back):
            index = block(half, offset(k), -(hop - 1 + back) * sign(side))
            return piece(self.buf, self.ssem, self.r2.at[half, side, hop - 1, k],
                         half, 2, hop, side, index)

        def begin(self):
            for half, side in FLOWS:
                self.first(half, side, 1, 0).start()

        def own(self, k):
            for half, side in FLOWS:
                self.second(half, side, 1, k, 0).start()

        def stage(self, hop, spread=True):
            for half, side in FLOWS:
                self.first(half, side, hop, 1).wait_recv()
                if hop < 4:
                    self.first(half, side, hop + 1, 0).start()
            if spread:
                self.spread(hop)

        def spread(self, hop):
            self.own(2 * hop - 1)
            if hop < 4:
                self.own(2 * hop)

        def forward(self, hop):
            def step(k, c):
                for half, side in FLOWS:
                    self.second(half, side, hop - 1, k, 1).wait_recv()
                    self.second(half, side, hop, k, 0).start()
                return c
            lax.fori_loop(0, RING, step, 0)

        def last(self):
            def step(k, c):
                for half, side in FLOWS:
                    self.second(half, side, 4, k, 1).wait_recv()
                return c
            lax.fori_loop(0, RING, step, 0)

        def drain(self):
            ref = self.buf.at[pl.ds(0, 63)]
            pltpu.make_async_remote_copy(
                src_ref=ref, dst_ref=ref, send_sem=self.ssem, recv_sem=self.r1.at[0, 0, 0],
                device_id=neighbour(0, 1, 0), device_id_type=MESH,
            ).wait_send()

    win = Gather(W, w_ssem, w_r1, w_r2)
    wout = Gather(Wo, o_ssem, o_r1, o_r2)

    win.begin()
    win.own(0)

    copies[4].wait()
    copies[5].wait()

    def norm_step(i, c):
        at = pl.ds(pl.multiple_of(i * 16, 16), 16)
        x = tok[at, :].astype(F32)
        scale = lax.rsqrt(jnp.mean(x * x, axis=-1, keepdims=True) + EPS)
        xn[at, :] = (x * scale * ng[...]).astype(BF16)
        return c

    lax.fori_loop(0, ROWS // 16, norm_step, 0)
    win.stage(1)

    lane = iota((1, 128), 1)
    freq = jnp.zeros((1, 128), F32)
    for i in range(32):
        freq = jnp.where(lax.rem(lane, 32) == i, F32(BASE ** (-2.0 * i / 64)), freq)
    position = (sp * ROWS + iota((ROWS, 128), 0)).astype(F32)
    angle = position * freq
    lane_full = iota((ROWS, 128), 1)
    low_half = lax.rem(lane_full, 64) < 32
    cosr[...] = jnp.cos(angle)
    sine = jnp.sin(angle)
    sinr[...] = jnp.where(low_half, -sine, sine)
    win.stage(2)

    for i in (6, 7):
        copies[i].wait()
    lane_n = iota((1, NST), 1)
    spread64 = (lax.rem(iota((64, NST), 1), 64) == iota((64, NST), 0)).astype(F32)
    own_group = iota((16, NST), 1) // 64 == iota((16, NST), 0)

    def as_row(ref):
        tiled = lax.dot_general(
            ref[...], spread64, (((1,), (0,)), ((), ())),
            precision=lax.Precision.HIGHEST, preferred_element_type=F32,
        )
        return jnp.sum(jnp.where(own_group, tiled, 0.0), axis=0, keepdims=True)

    lam_re = -as_row(dec)
    lam_im = as_row(rot)
    step_log = jnp.zeros((1, NST), F32)
    for g in range(16):
        step_log = jnp.where(lane_n // 64 == g, ls_s[g], step_log)
    delta = jnp.exp(step_log)
    modulus = jnp.exp(lam_re * delta)
    pr = modulus * jnp.cos(lam_im * delta)
    pi = modulus * jnp.sin(lam_im * delta)
    less = pr - 1.0
    den = lam_re * lam_re + lam_im * lam_im
    prow[0:1, :] = (less * lam_re + pi * lam_im) / den
    prow[1:2, :] = (pi * lam_re - less * lam_im) / den
    ar, ai = pr, pi
    for k in range(16):
        pw[0, k : k + 1, :] = ar
        pw[1, k : k + 1, :] = ai
        if k < 15:
            ar, ai = cmul(ar, ai, pr, pi)
    prow[2:3, :] = ar
    prow[3:4, :] = ai
    for _ in range(3):
        ar, ai = cmul(ar, ai, ar, ai)
    prow[4:5, :] = ar
    prow[5:6, :] = ai
    for _ in range(3):
        ar, ai = cmul(ar, ai, ar, ai)
    prow[6:7, :] = ar
    prow[7:8, :] = ai
    win.stage(3)

    for i in (8, 9, 10, 11):
        copies[i].wait()
    spread64b = spread64.astype(BF16)
    own_block = iota((256, NST), 0) // 16 == iota((256, NST), 1) // 64

    def diagonal(dst, at, value):
        for part, value in enumerate(split(value.reshape(256, 64))):
            dst[at + part] = jnp.where(own_block, nn(value, spread64b), 0.0).astype(BF16)

    diagonal(BDi, 0, inre[...])
    diagonal(BDi, 2, inim[...])
    win.stage(4)
    diagonal(BDo, 0, outre[...])
    diagonal(BDo, 2, -outim[...])

    for i in (12, 13, 14, 15):
        copies[i].wait()

    win.forward(2)
    wout.begin()
    win.forward(3)
    wout.stage(1, False)
    win.forward(4)
    wout.stage(2, False)
    wout.own(0)
    wout.spread(1)
    wout.spread(2)
    win.last()
    wout.stage(3)

    def project(i, c):
        wide = W[pl.ds(pl.multiple_of(i * 8, 8), 8)].reshape(512, NIN)
        xs = xn[:, pl.ds(pl.multiple_of(i * 512, 512), 512)]
        part = nn(xs, wide)

        @pl.when(i == 0)
        def _():
            qkvs[...] = part

        @pl.when(i > 0)
        def _():
            qkvs[...] += part

        return c

    lax.fori_loop(0, RING, project, 0)
    wout.stage(4)

    def swapped(x):
        return jnp.where(low_half, pltpu.roll(x, 96, 1), pltpu.roll(x, 32, 1))

    kv = qkvs[:, 512:640]
    key_lane = lane_full < 64
    kv = kv * jnp.where(key_lane, cosr[...], 1.0) + swapped(kv) * jnp.where(
        key_lane, sinr[...], 0.0
    )
    KVb[1] = kv.astype(BF16)
    u = qkvs[:, 256:512].astype(BF16)
    permute = (
        iota((ROWS, ROWS), 1)
        == 16 * lax.rem(iota((ROWS, ROWS), 0), 8) + iota((ROWS, ROWS), 0) // 8
    ).astype(F32).astype(BF16)
    up = nn(permute, u).astype(BF16)
    kv_copy = pltpu.make_async_remote_copy(
        src_ref=KVb.at[1], dst_ref=KVb.at[0], send_sem=kv_ss, recv_sem=kv_rs,
        device_id=(after, t), device_id_type=MESH,
    )
    kv_copy.start()

    Sr[...] = nn(up, BDi[0]) + nn(up, BDi[1])
    Si[...] = nn(up, BDi[2]) + nn(up, BDi[3])
    fr, fi = prow[0:1, :], prow[1:2, :]
    pr, pi = pw[0, 0:1, :], pw[1, 0:1, :]
    sr = jnp.zeros((8, NST), F32)
    si = jnp.zeros((8, NST), F32)
    for i in range(16):
        at = slice(8 * i, 8 * i + 8)
        br, bi = cmul(fr, fi, Sr[at, :], Si[at, :])
        sr, si = cmul(pr, pi, sr, si)
        sr, si = sr + br, si + bi
        Sr[at, :] = sr
        Si[at, :] = si
    Er[...] = sr
    Ei[...] = si
    qr, qi = prow[2:3, :], prow[3:4, :]
    cr = jnp.zeros((1, NST), F32)
    ci = jnp.zeros((1, NST), F32)
    for j in range(8):
        cr, ci = cmul(qr, qi, cr, ci)
        cr, ci = cr + Er[j : j + 1, :], ci + Ei[j : j + 1, :]
    CY[y, 0:1, :] = cr
    CY[y, 1:2, :] = ci
    for pair in range(2):
        x = qkvs[:, 128 * pair : 128 * pair + 128]
        qb[:, 128 * pair : 128 * pair + 128] = (x * cosr[...] + swapped(x) * sinr[...]).astype(BF16)

    def carry_copy(buf, ss, rs, at, peer):
        return pltpu.make_async_remote_copy(
            src_ref=buf.at[at], dst_ref=buf.at[at], send_sem=ss, recv_sem=rs,
            device_id=peer, device_id_type=MESH,
        )

    def carry_all(buf, ss, rs):
        return carry_copy(buf, ss, rs, pl.ds(0, 7), peers[0])

    for j in range(1, RING):
        carry_copy(CY, cy_ss, cy_rs, y, (z * RING + ring(y, j), t)).start()
    wout.forward(2)

    kv_copy.wait_recv()
    both = KVb[...].reshape(2 * ROWS, 128).astype(F32)
    turned = pltpu.roll(both, 64, 1)
    first_half = iota((2 * ROWS, 128), 1) < 64
    k_low = jnp.where(first_half, both, 0.0).astype(BF16)
    k_high = jnp.where(first_half, 0.0, turned).astype(BF16)
    v_low = jnp.where(first_half, turned, 0.0).astype(BF16)
    v_high = jnp.where(first_half, 0.0, both).astype(BF16)
    gap = iota((ROWS, 2 * ROWS), 0) + ROWS - iota((ROWS, 2 * ROWS), 1)
    key_at = sp * ROWS - ROWS + iota((ROWS, 2 * ROWS), 1)
    visible = (gap >= 0) & (gap < ROWS) & (key_at >= 0)

    def attend(pair):
        q = qb[:, 128 * pair : 128 * pair + 128]
        total = None
        for side, (k, v) in enumerate(((k_low, v_low), (k_high, v_high))):
            score = jnp.where(visible, nt(q, k) * 0.125, -jnp.inf)
            sink = sink_s[2 * pair + side]
            top = jnp.maximum(jnp.max(score, axis=-1, keepdims=True), sink)
            e = jnp.exp(score - top)
            weight = e / (jnp.sum(e, axis=-1, keepdims=True) + jnp.exp(sink - top))
            part = nn(weight.astype(BF16), v)
            total = part if total is None else total + part
        M[:, 128 * pair : 128 * pair + 128] = total.astype(BF16)

    attend(0)

    carry_all(CY, cy_ss, cy_rs).wait_recv()
    br, bi = prow[4:5, :], prow[5:6, :]
    cr = jnp.zeros((1, NST), F32)
    ci = jnp.zeros((1, NST), F32)
    rowr, rowi = cr, ci
    wr, wi = cr + 1.0, ci
    for j in range(RING):
        keep = jnp.where(y == j, 1.0, 0.0).astype(F32)
        rowr = rowr + keep * cr
        rowi = rowi + keep * ci
        cr, ci = cmul(br, bi, cr, ci)
        cr, ci = cr + CY[j, 0:1, :], ci + CY[j, 1:2, :]
        go = jnp.where(y > j, 1.0, 0.0).astype(F32)
        nr, ni = cmul(br, bi, wr, wi)
        wr = wr + go * (nr - wr)
        wi = wi + go * (ni - wi)
    CZ[z, 0:1, :] = cr
    CZ[z, 1:2, :] = ci
    Cr[0:1, :] = rowr
    Ci[0:1, :] = rowi
    Cr[1:2, :] = wr
    Ci[1:2, :] = wi
    for j in range(1, RING):
        carry_copy(CZ, cz_ss, cz_rs, z, (ring(z, j) * RING + y, t)).start()
    wout.forward(3)
    attend(1)

    carry_all(CZ, cz_ss, cz_rs).wait_recv()
    br, bi = prow[6:7, :], prow[7:8, :]
    cr = jnp.zeros((1, NST), F32)
    ci = jnp.zeros((1, NST), F32)
    for j in range(RING - 1):
        go = jnp.where(z > j, 1.0, 0.0).astype(F32)
        nr, ni = cmul(br, bi, cr, ci)
        nr, ni = nr + CZ[j, 0:1, :], ni + CZ[j, 1:2, :]
        cr = go * nr + (1.0 - go) * cr
        ci = go * ni + (1.0 - go) * ci
    cr, ci = cmul(Cr[1:2, :], Ci[1:2, :], cr, ci)
    cr, ci = cr + Cr[0:1, :], ci + Ci[0:1, :]
    for j in range(8):
        Cr[j : j + 1, :] = cr
        Ci[j : j + 1, :] = ci
        cr, ci = cmul(qr, qi, cr, ci)
        cr, ci = cr + Er[j : j + 1, :], ci + Ei[j : j + 1, :]
    cr, ci = Cr[...], Ci[...]
    for i in range(16):
        at = slice(8 * i, 8 * i + 8)
        gr, gi = cmul(pw[0, i : i + 1, :], pw[1, i : i + 1, :], cr, ci)
        Sr[at, :] = Sr[at, :] + gr
        Si[at, :] = Si[at, :] + gi
    total = up.astype(F32) * sg[...]
    for j, ref in ((0, Sr), (2, Si)):
        high, low = split(ref[...])
        total = total + nt(high, BDo[j]) + nt(low, BDo[j]) + nt(high, BDo[j + 1])
    mixed = jax.nn.gelu(total).astype(BF16)
    M[:, 256:512] = lax.dot_general(
        permute, mixed, (((0,), (0,)), ((), ())), preferred_element_type=F32
    ).astype(BF16)

    def chunk(half, a):
        lines = [
            Wo[(8 * j + a) if half == 0 else (8 * a + j), 32 * half : 32 * half + 32]
            for j in range(RING)
        ]
        part = nt(M[...], jnp.concatenate(lines, axis=0)).astype(BF16)
        at = a + RING * half
        Pb[at] = part.reshape(TP, 16, 256)
        R[t, at] = Pb[at, t]
        return at

    def owner_copy(at, j):
        to = lax.rem(t + j, TP)
        return pltpu.make_async_remote_copy(
            src_ref=Pb.at[at, to], dst_ref=R.at[t, at], send_sem=rs_ss, recv_sem=rs_rs,
            device_id=(sp, to), device_id_type=MESH,
        )

    def chunks(items):
        made = [chunk(half, a) for half, a in items]
        for at in made:
            for j in range(1, TP):
                owner_copy(at, j).start()

    def at_hop(hop):
        return [(0, ring(y, hop)), (0, ring(y, -hop)), (1, ring(z, hop)), (1, ring(z, -hop))]

    chunks([(0, y), (1, z)] + at_hop(1))
    wout.forward(4)
    chunks(at_hop(2))
    chunks(at_hop(3))
    wout.last()
    chunks([(0, ring(y, 4)), (1, ring(z, 4))])

    kv_copy.wait_send()
    carry_all(CY, cy_ss, cy_rs).wait_send()
    carry_all(CZ, cz_ss, cz_rs).wait_send()
    win.drain()
    wout.drain()
    whole = pltpu.make_async_remote_copy(
        src_ref=R.at[pl.ds(0, 7)], dst_ref=R.at[pl.ds(0, 7)], send_sem=rs_ss, recv_sem=rs_rs,
        device_id=peers[0], device_id_type=MESH,
    )
    whole.wait_send()
    whole.wait_recv()

    square = jnp.zeros((16, 1), F32)
    sums = []
    for at in range(2 * RING):
        total = R[0, at].astype(F32)
        for j in range(1, TP):
            total = total + R[j, at].astype(F32)
        sums.append(total)
        square = square + jnp.sum(total * total, axis=-1, keepdims=True)
    scale = lax.rsqrt(square * (1.0 / D) + EPS)
    quarter = iota((16, 128), 1) // 32
    for n in range(32):
        zz, y0 = n // 4, 2 * (n % 4)
        tile = None
        pieces = ((sums[y0], zz), (sums[RING + zz], y0), (sums[y0 + 1], zz), (sums[RING + zz], y0 + 1))
        for place, (source, at) in enumerate(pieces):
            part = source[:, 128 * (at // 4) : 128 * (at // 4) + 128]
            shift = (32 * place - 32 * (at % 4)) % 128
            if shift:
                part = pltpu.roll(part, shift, 1)
            tile = part if tile is None else jnp.where(quarter == place, part, tile)
        cols = slice(128 * n, 128 * n + 128)
        out_ref[:, cols] = (tile * scale * og[:, cols]).astype(BF16)


def body(
    tokens, norm_gain, w_query, w_key, w_value, w_state_in, sink_logit, decay_rate, rotation,
    log_step, in_re, in_im, out_re, out_im, skip_gain, w_attn_out, w_state_out, out_gain,
):
    vm, dma = pltpu.VMEM, pltpu.SemaphoreType.DMA
    spec = pl.BlockSpec(memory_space=pl.ANY)
    specs = [spec] * 18
    specs[6] = specs[9] = pl.BlockSpec(memory_space=pltpu.SMEM)
    return pl.pallas_call(
        kernel,
        out_shape=jax.ShapeDtypeStruct((16, D), BF16),
        in_specs=specs,
        out_specs=pl.BlockSpec(memory_space=pltpu.VMEM),
        scratch_shapes=[
            vm((64, 64, NIN), BF16),
            vm((64, 64, 512), BF16),
            vm((ROWS, D), BF16),
            vm((ROWS, D), BF16),
            vm((64, 64), BF16),
            vm((64, 64), BF16),
            vm((1, D), F32),
            vm((1, D), F32),
            vm((1, 256), F32),
            vm((16, 64), F32),
            vm((16, 64), F32),
            vm((16, 16, 64), F32),
            vm((16, 16, 64), F32),
            vm((16, 16, 64), F32),
            vm((16, 16, 64), F32),
            vm((ROWS, NIN), F32),
            vm((ROWS, 128), F32),
            vm((ROWS, 128), F32),
            vm((8, NST), F32),
            vm((2, 16, NST), F32),
            vm((4, 256, NST), BF16),
            vm((4, 256, NST), BF16),
            vm((ROWS, NST), F32),
            vm((ROWS, NST), F32),
            vm((8, NST), F32),
            vm((8, NST), F32),
            vm((8, NST), F32),
            vm((8, NST), F32),
            vm((RING, 2, NST), F32),
            vm((RING, 2, NST), F32),
            vm((2, ROWS, 128), BF16),
            vm((ROWS, 256), BF16),
            vm((ROWS, 512), BF16),
            vm((2 * RING, TP, 16, 256), BF16),
            vm((TP, 2 * RING, 16, 256), BF16),
            dma((16,)),
            dma, dma((2, 2, 4)), dma((2, 2, 4, RING)),
            dma, dma((2, 2, 4)), dma((2, 2, 4, RING)),
            dma, dma, dma, dma, dma, dma, dma, dma,
        ],
        compiler_params=pltpu.CompilerParams(collective_id=0, has_side_effects=True),
    )(
        tokens, norm_gain.reshape(1, D), w_query, w_key, w_value, w_state_in, sink_logit,
        decay_rate, rotation, log_step, in_re.transpose(0, 2, 1), in_im.transpose(0, 2, 1),
        out_re, out_im, skip_gain.reshape(1, 256), w_attn_out.T, w_state_out.T, out_gain.reshape(1, D),
    )


def solution(mesh):
    return jax.shard_map(
        body,
        mesh=mesh,
        in_specs=(
            P("sp", None),
            P(),
            P("sp", "tp"),
            P("sp", "tp"),
            P("sp", "tp"),
            P("sp", "tp"),
            P("tp"),
            P("tp", None),
            P("tp", None),
            P("tp"),
            P("tp", None, None),
            P("tp", None, None),
            P("tp", None, None),
            P("tp", None, None),
            P("tp"),
            P("tp", "sp"),
            P("tp", "sp"),
            P(),
        ),
        out_specs=P(("sp", "tp"), None),
        check_vma=False,
    )
```

time: 315 us -> 87.6 us (0.28)
  local copies, waits for them, and re-layouts: 116 us -> 1.57 us
  waiting for transfers between devices: 98.9 us -> 0 us
  Pallas kernels: 0 us -> 85.9 us
  other arithmetic: 29 us -> 0 us
  blocking collectives: 25.6 us -> 0 us
  matrix products: 16.3 us -> 0 us
  between operations: 15.7 us -> 0.01 us
  starting transfers between devices: 11.9 us -> 0 us
    slice x88 -> x0, local copies, waits for them, and re-layouts: 96.7 us -> none  [the longest x47 82.6 us: local_states(): lax.associative_scan(chain_link, (decay_re, decay_im, push_re, push_im),...]
    pallas_call x0 -> x1, Pallas kernels: none -> 85.9 us  [body(): pl.pallas_call(kernel, out_shape=jax.ShapeDtypeStruct((16, D), BF16), in_...]
    all_gather x2 -> x0, waiting for transfers between devices: 81.6 us -> none  [the longest x1 81.6 us: side_by_side(): lax.all_gather(both, axis, axis=dim, tiled=True)]
    all_to_all x1 -> x0, blocking collectives: 25.6 us -> none  [sum_at_owner(): lax.all_to_all(blocks, axis, split_axis=0, concat_axis=0, tiled=True)]
    all_to_all x1 -> x0, waiting for transfers between devices: 17.2 us -> none  [copy_for_each(): lax.all_to_all(jnp.broadcast_to(value[None], (size, *value.shape)), axis,...]
    dot_general x12 -> x0, matrix products: 16.3 us -> none  [the longest x4 9.16 us: add_pieces(): lax.dot_general(normed_cols, weight_piece, (((0,), (0,)), ((), ())), pref...]
    add x52 -> x0, other arithmetic: 12.3 us -> none  [the longest x13 4.85 us: chain_link(): late_are * early_bim + late_aim * early_bre + late_bim]
    pad x48 -> x0, local copies, waits for them, and re-layouts: 8.91 us -> none  [local_states(): lax.associative_scan(chain_link, (decay_re, decay_im, push_re, push_im),...]
  transfers between devices with their start and end apart: 4 -> 0, of which waited for: 2 -> 0; matrix products, arithmetic and copies ran while one was open for 42% -> 0% of each run, Pallas kernels for 0% -> 0%
where the time goes in v1:
time: 87.6 us; the launch traced here: 87.4 us
  Pallas kernels  85.9 us (98%)
  local copies, waits for them, and re-layouts  1.57 us (2%)
    pallas_call x1, Pallas kernels, body(): pl.pallas_call(kernel, out_shape=jax.ShapeDtypeStruct((16, D), BF16), in_...  85.9 us

profile of v1, /device:TPU:1, one launch (start us, length us, event | category | flops | bytes accessed | tf_op | source)
XLA Modules:
  0.0 87.4 jit_solution(6275124994537181901)
XLA Ops:
  0.0 85.9 %shard_map.172 = bf16[16,4096]{1,0:T(8,128)(2,1)} custom-call(bf16[128,4096]{1,0:T(8,128)(2,1)} %tok_h.1, f32[1,4096]{1,0:T(1,128)} %bitcast.11, bf16[64,256]{1,0:T(8,128)(2,1)} %wq_h.1, bf16[64,64]{1,0:T(8,128)(2,1)} %wk_h.1, bf16[64,64]{1,0:T(8,128)(2,1)} %wv_h.1, bf16[64,256]{1,0:T(8,128)(2,1)} %ws_h.1, f32[4]{0:T(128)} %sink_s.1, f32[16,64]{1,0:T(8,128)} %dec_h.1, ...), custom_call_target="tpu_custom_call" | custom-call | tf_op jit(solution)/shard_map/pallas_call | solution.py:541
  85.9 1.6 %copy.20 = bf16[16,4096]{1,0:T(8,128)(2,1)} copy(bf16[16,4096]{1,0:T(8,128)(2,1)} %shard_map.172) | data formatting | bytes 262144

commit v2 on v1

--- a/solution.py
+++ b/solution.py
@@ -14,6 +14,7 @@
 BASE = 500000.0
 RING = 8
 TP = 8
+CHIPS = 4
 ROWS = 128
 D = 4096
 NIN = 640
@@ -47,22 +48,42 @@
 
 
 def kernel(
-    tok_h, ng_h, wq_h, wk_h, wv_h, ws_h, sink_s, dec_h, rot_h, ls_s,
+    tok_h, ng_h, wq_h, wk_h, wv_h, ws_h, sink_h, dec_h, rot_h, ls_h,
     inre_h, inim_h, outre_h, outim_h, sg_h, wa_h, wso_h, og_h,
     out_ref,
-    W, Wo, tok, xn, kw, vw, ng, og, sg, dec, rot, inre, inim, outre, outim,
-    qkvs, cosr, sinr, prow, pw, BDi, BDo, Sr, Si, Er, Ei, Cr, Ci, CY, CZ, KVb, qb, M, Pb, R,
+    W, Wo, tok, xn, xh, kw, vw, sink_s, ls_s, ng, og, sg, dec, rot, inre, inim, outre, outim,
+    qkvs, cosr, sinr, prow, pw, BDi, BDo, Sr, Si, Er, Ei, Cr, Ci, CY, CZ, KVb, qb, M, PP, PR, Pb, R, T,
     lsem, w_ssem, w_r1, w_r2, o_ssem, o_r1, o_r2, kv_ss, kv_rs, cy_ss, cy_rs, cz_ss, cz_rs,
-    rs_ss, rs_rs,
+    rs_ss, rs_rs, tw_ss, tw_rs,
 ):
     sp = lax.axis_index("sp")
     t = lax.axis_index("tp")
     z = sp // RING
     y = lax.rem(sp, RING)
 
-    local = [
-        (wq_h, W.at[sp, :, pl.ds(0, 256)]),
-        (ws_h, W.at[sp, :, pl.ds(256, 256)]),
+    chip = t // 2
+    core = lax.rem(t, 2)
+    twin = (sp, t + 1 - 2 * core)
+    barrier = pltpu.get_barrier_semaphore()
+    after = lax.rem(sp + 1, RING * RING)
+    before = lax.rem(sp + RING * RING - 1, RING * RING)
+    peers = [(z * RING + ring(y, j), t) for j in range(1, RING)]
+    peers += [(ring(z, j) * RING + y, t) for j in range(1, RING)]
+    peers += [(sp, lax.rem(t + 2 * j, TP)) for j in range(1, CHIPS)]
+    peers += [twin]
+    peers += [(after, t), (before, t)]
+    for peer in peers:
+        pl.semaphore_signal(barrier, inc=1, device_id=peer, device_id_type=MESH)
+
+    mine = (y * RING + z, z * RING + y)
+    local = []
+    for half in (0, 1):
+        at = pl.ds(32 * half, 32)
+        local += [
+            (wq_h.at[at], W.at[half, mine[half], :, pl.ds(0, 256)]),
+            (ws_h.at[at], W.at[half, mine[half], :, pl.ds(256, 256)]),
+        ]
+    local += [
         (wk_h, kw),
         (wv_h, vw),
         (tok_h, tok),
@@ -73,38 +94,35 @@
         (inim_h, inim),
         (outre_h, outre),
         (outim_h, outim),
-        (wa_h, Wo.at[sp, :, pl.ds(0, 256)]),
-        (wso_h, Wo.at[sp, :, pl.ds(256, 256)]),
         (sg_h, sg),
         (og_h, og),
+        (sink_h, sink_s),
+        (ls_h, ls_s),
     ]
+    for half in (0, 1):
+        at = pl.ds(32 * half, 32)
+        local += [
+            (wa_h.at[at], Wo.at[half, mine[half], :, pl.ds(0, 256)]),
+            (wso_h.at[at], Wo.at[half, mine[half], :, pl.ds(256, 256)]),
+        ]
     copies = [pltpu.make_async_copy(a, b, lsem.at[i]) for i, (a, b) in enumerate(local)]
     for c in copies:
         c.start()
 
-    barrier = pltpu.get_barrier_semaphore()
-    after = lax.rem(sp + 1, RING * RING)
-    before = lax.rem(sp + RING * RING - 1, RING * RING)
-    peers = [(z * RING + ring(y, j), t) for j in range(1, RING)]
-    peers += [(ring(z, j) * RING + y, t) for j in range(1, RING)]
-    peers += [(sp, lax.rem(t + j, TP)) for j in range(1, TP)]
-    peers += [(after, t), (before, t)]
-    for peer in peers:
-        pl.semaphore_signal(barrier, inc=1, device_id=peer, device_id_type=MESH)
-
-    for i in range(4):
+    for i in range(6):
         copies[i].wait()
     lane64 = iota((64, 128), 1)
     row64 = iota((64, 128), 0)
     to_low = (lane64 == row64).astype(F32).astype(BF16)
     to_high = (lane64 == row64 + 64).astype(F32).astype(BF16)
-    W[sp, :, 512:640] = (nn(kw[...], to_low) + nn(vw[...], to_high)).astype(BF16)
+    kv_part = (nn(kw[...], to_low) + nn(vw[...], to_high)).astype(BF16)
+    W[0, mine[0], :, 512:640] = kv_part[:32]
+    W[1, mine[1], :, 512:640] = kv_part[32:]
     pl.semaphore_wait(barrier, len(peers))
 
     def block(half, d1, d2):
-        if half == 0:
-            return ring(z, d1) * RING + ring(y, d2)
-        return ring(z, d2) * RING + ring(y, d1)
+        first, second = (z, y) if half == 0 else (y, z)
+        return ring(second, d2) * RING + ring(first, d1)
 
     def neighbour(half, phase, side):
         step = 1 if side == 0 else -1
@@ -112,13 +130,11 @@
             return (ring(z, step) * RING + y, t)
         return (z * RING + ring(y, step), t)
 
-    def rows(half, hop, side):
-        if hop < 4:
-            return pl.ds(32 * half, 32)
-        return pl.ds(32 * half + 16 * side, 16)
+    def rows(hop, side):
+        return pl.ds(0, 32) if hop < 4 else pl.ds(16 * side, 16)
 
     def piece(buf, ssem, rsem, half, phase, hop, side, index):
-        ref = buf.at[index, rows(half, hop, side)]
+        ref = buf.at[half, index, rows(hop, side)]
         return pltpu.make_async_remote_copy(
             src_ref=ref, dst_ref=ref, send_sem=ssem, recv_sem=rsem,
             device_id=neighbour(half, phase, side), device_id_type=MESH,
@@ -167,13 +183,13 @@
             if hop < 4:
                 self.own(2 * hop)
 
-        def forward(self, hop):
+        def forward(self, hop, begin=0, end=RING):
             def step(k, c):
                 for half, side in FLOWS:
                     self.second(half, side, hop - 1, k, 1).wait_recv()
                     self.second(half, side, hop, k, 0).start()
                 return c
-            lax.fori_loop(0, RING, step, 0)
+            lax.fori_loop(begin, end, step, 0)
 
         def last(self):
             def step(k, c):
@@ -183,7 +199,7 @@
             lax.fori_loop(0, RING, step, 0)
 
         def drain(self):
-            ref = self.buf.at[pl.ds(0, 63)]
+            ref = self.buf.at[:, pl.ds(0, 63)]
             pltpu.make_async_remote_copy(
                 src_ref=ref, dst_ref=ref, send_sem=self.ssem, recv_sem=self.r1.at[0, 0, 0],
                 device_id=neighbour(0, 1, 0), device_id_type=MESH,
@@ -192,11 +208,14 @@
     win = Gather(W, w_ssem, w_r1, w_r2)
     wout = Gather(Wo, o_ssem, o_r1, o_r2)
 
-    win.begin()
-    win.own(0)
-
-    copies[4].wait()
-    copies[5].wait()
+    for i in (18, 19, 20, 21):
+        copies[i].wait()
+    for gather in (win, wout):
+        gather.begin()
+        gather.own(0)
+
+    copies[6].wait()
+    copies[7].wait()
 
     def norm_step(i, c):
         at = pl.ds(pl.multiple_of(i * 16, 16), 16)
@@ -207,6 +226,7 @@
 
     lax.fori_loop(0, ROWS // 16, norm_step, 0)
     win.stage(1)
+    win.forward(2, 0, 1)
 
     lane = iota((1, 128), 1)
     freq = jnp.zeros((1, 128), F32)
@@ -220,8 +240,33 @@
     sine = jnp.sin(angle)
     sinr[...] = jnp.where(low_half, -sine, sine)
     win.stage(2)
-
-    for i in (6, 7):
+    wout.stage(1, False)
+    win.forward(2, 1, 2)
+
+    lane128 = iota((ROWS, 128), 1) // 32
+    source = iota((512, 256), 0)
+    target = iota((512, 256), 1)
+    spot = 64 * (target // 32) + lax.rem(target, 32)
+    picks = [(source == spot + 32 * half).astype(F32).astype(BF16) for half in (0, 1)]
+    for i in range(RING):
+        xh[1, i] = nn(xn[:, 512 * i : 512 * i + 512], picks[1]).astype(BF16)
+    for group in range(2):
+        rolled = []
+        for i in range(4):
+            at = 512 * (4 * group + i)
+            part = nn(xn[:, at : at + 512], picks[0])
+            rolled.append((part[:, :128], part[:, 128:]))
+        for j in range(RING):
+            tile = None
+            for i in range(4):
+                part = rolled[i][j // 4]
+                shift = 32 * ((i - j) % 4)
+                if shift:
+                    part = pltpu.roll(part, shift, 1)
+                tile = part if tile is None else jnp.where(lane128 == i, part, tile)
+            xh[0, j, :, 128 * group : 128 * group + 128] = tile.astype(BF16)
+
+    for i in (8, 9, 17):
         copies[i].wait()
     lane_n = iota((1, NST), 1)
     spread64 = (lax.rem(iota((64, NST), 1), 64) == iota((64, NST), 0)).astype(F32)
@@ -264,8 +309,9 @@
     prow[6:7, :] = ar
     prow[7:8, :] = ai
     win.stage(3)
-
-    for i in (8, 9, 10, 11):
+    win.forward(2, 2, 4)
+
+    for i in (10, 11, 12, 13):
         copies[i].wait()
     spread64b = spread64.astype(BF16)
     own_block = iota((256, NST), 0) // 16 == iota((256, NST), 1) // 64
@@ -277,41 +323,45 @@
     diagonal(BDi, 0, inre[...])
     diagonal(BDi, 2, inim[...])
     win.stage(4)
+    win.forward(2, 4, 6)
     diagonal(BDo, 0, outre[...])
     diagonal(BDo, 2, -outim[...])
 
-    for i in (12, 13, 14, 15):
+    for i in (14, 15, 16):
         copies[i].wait()
-
-    win.forward(2)
-    wout.begin()
-    win.forward(3)
-    wout.stage(1, False)
-    win.forward(4)
+    win.forward(2, 6, 8)
     wout.stage(2, False)
-    wout.own(0)
-    wout.spread(1)
-    wout.spread(2)
+
+    def project(half, a, fresh=False):
+        wide = W[half, pl.ds(pl.multiple_of(a * RING, RING), RING)].reshape(256, NIN)
+        part = nn(xh[half, a], wide)
+        qkvs[...] = part if fresh else qkvs[...] + part
+
+    def at_hop(hop):
+        if hop == 0:
+            return [(0, y), (1, z)]
+        if hop == 4:
+            return [(0, ring(y, 4)), (1, ring(z, 4))]
+        return [(0, ring(y, hop)), (0, ring(y, -hop)), (1, ring(z, hop)), (1, ring(z, -hop))]
+
+    def projects(hop):
+        for n, (half, a) in enumerate(at_hop(hop)):
+            project(half, a, hop == 0 and n == 0)
+
+    projects(0)
+    win.forward(3, 0, 4)
+    projects(1)
+    win.forward(3, 4, 8)
+    wout.stage(3, False)
+    win.forward(4, 0, 4)
+    projects(2)
+    win.forward(4, 4, 8)
+    wout.stage(4, False)
+    for k in range(1, RING):
+        wout.own(k)
+    projects(3)
     win.last()
-    wout.stage(3)
-
-    def project(i, c):
-        wide = W[pl.ds(pl.multiple_of(i * 8, 8), 8)].reshape(512, NIN)
-        xs = xn[:, pl.ds(pl.multiple_of(i * 512, 512), 512)]
-        part = nn(xs, wide)
-
-        @pl.when(i == 0)
-        def _():
-            qkvs[...] = part
-
-        @pl.when(i > 0)
-        def _():
-            qkvs[...] += part
-
-        return c
-
-    lax.fori_loop(0, RING, project, 0)
-    wout.stage(4)
+    projects(4)
 
     def swapped(x):
         return jnp.where(low_half, pltpu.roll(x, 96, 1), pltpu.roll(x, 32, 1))
@@ -322,18 +372,20 @@
         key_lane, sinr[...], 0.0
     )
     KVb[1] = kv.astype(BF16)
+    kv_copy = pltpu.make_async_remote_copy(
+        src_ref=KVb.at[1], dst_ref=KVb.at[0], send_sem=kv_ss, recv_sem=kv_rs,
+        device_id=(after, t), device_id_type=MESH,
+    )
+    kv_copy.start()
+
+    wout.forward(2, 0, 2)
+
     u = qkvs[:, 256:512].astype(BF16)
     permute = (
         iota((ROWS, ROWS), 1)
         == 16 * lax.rem(iota((ROWS, ROWS), 0), 8) + iota((ROWS, ROWS), 0) // 8
     ).astype(F32).astype(BF16)
     up = nn(permute, u).astype(BF16)
-    kv_copy = pltpu.make_async_remote_copy(
-        src_ref=KVb.at[1], dst_ref=KVb.at[0], send_sem=kv_ss, recv_sem=kv_rs,
-        device_id=(after, t), device_id_type=MESH,
-    )
-    kv_copy.start()
-
     Sr[...] = nn(up, BDi[0]) + nn(up, BDi[1])
     Si[...] = nn(up, BDi[2]) + nn(up, BDi[3])
     fr, fi = prow[0:1, :], prow[1:2, :]
@@ -357,9 +409,6 @@
         cr, ci = cr + Er[j : j + 1, :], ci + Ei[j : j + 1, :]
     CY[y, 0:1, :] = cr
     CY[y, 1:2, :] = ci
-    for pair in range(2):
-        x = qkvs[:, 128 * pair : 128 * pair + 128]
-        qb[:, 128 * pair : 128 * pair + 128] = (x * cosr[...] + swapped(x) * sinr[...]).astype(BF16)
 
     def carry_copy(buf, ss, rs, at, peer):
         return pltpu.make_async_remote_copy(
@@ -372,7 +421,11 @@
 
     for j in range(1, RING):
         carry_copy(CY, cy_ss, cy_rs, y, (z * RING + ring(y, j), t)).start()
-    wout.forward(2)
+    wout.forward(2, 2, 6)
+    for pair in range(2):
+        x = qkvs[:, 128 * pair : 128 * pair + 128]
+        qb[:, 128 * pair : 128 * pair + 128] = (x * cosr[...] + swapped(x) * sinr[...]).astype(BF16)
+    wout.forward(2, 6, 8)
 
     kv_copy.wait_recv()
     both = KVb[...].reshape(2 * ROWS, 128).astype(F32)
@@ -399,8 +452,8 @@
             total = part if total is None else total + part
         M[:, 128 * pair : 128 * pair + 128] = total.astype(BF16)
 
+
     attend(0)
-
     carry_all(CY, cy_ss, cy_rs).wait_recv()
     br, bi = prow[4:5, :], prow[5:6, :]
     cr = jnp.zeros((1, NST), F32)
@@ -425,8 +478,9 @@
     Ci[1:2, :] = wi
     for j in range(1, RING):
         carry_copy(CZ, cz_ss, cz_rs, z, (ring(z, j) * RING + y, t)).start()
-    wout.forward(3)
+
     attend(1)
+    wout.forward(3, 0, 6)
 
     carry_all(CZ, cz_ss, cz_rs).wait_recv()
     br, bi = prow[6:7, :], prow[7:8, :]
@@ -451,6 +505,7 @@
         gr, gi = cmul(pw[0, i : i + 1, :], pw[1, i : i + 1, :], cr, ci)
         Sr[at, :] = Sr[at, :] + gr
         Si[at, :] = Si[at, :] + gi
+    wout.forward(3, 6, 8)
     total = up.astype(F32) * sg[...]
     for j, ref in ((0, Sr), (2, Si)):
         high, low = split(ref[...])
@@ -461,67 +516,96 @@
     ).astype(BF16)
 
     def chunk(half, a):
-        lines = [
-            Wo[(8 * j + a) if half == 0 else (8 * a + j), 32 * half : 32 * half + 32]
-            for j in range(RING)
-        ]
-        part = nt(M[...], jnp.concatenate(lines, axis=0)).astype(BF16)
+        wide = Wo[half, pl.ds(pl.multiple_of(a * RING, RING), RING)].reshape(256, 512)
+        part = nt(M[...], wide).reshape(CHIPS, 2, 16, 256)
         at = a + RING * half
-        Pb[at] = part.reshape(TP, 16, 256)
-        R[t, at] = Pb[at, t]
+        PP[0, at] = part[:, 0]
+        PP[1, at] = part[:, 1]
         return at
 
-    def owner_copy(at, j):
-        to = lax.rem(t + j, TP)
-        return pltpu.make_async_remote_copy(
-            src_ref=Pb.at[at, to], dst_ref=R.at[t, at], send_sem=rs_ss, recv_sem=rs_rs,
-            device_id=(sp, to), device_id_type=MESH,
-        )
-
-    def chunks(items):
+    def make(batch, items):
         made = [chunk(half, a) for half, a in items]
         for at in made:
-            for j in range(1, TP):
-                owner_copy(at, j).start()
-
-    def at_hop(hop):
-        return [(0, ring(y, hop)), (0, ring(y, -hop)), (1, ring(z, hop)), (1, ring(z, -hop))]
-
-    chunks([(0, y), (1, z)] + at_hop(1))
-    wout.forward(4)
-    chunks(at_hop(2))
-    chunks(at_hop(3))
+            pltpu.make_async_remote_copy(
+                src_ref=PP.at[1 - core, at], dst_ref=PR.at[at], send_sem=tw_ss,
+                recv_sem=tw_rs.at[batch], device_id=twin, device_id_type=MESH,
+            ).start()
+        return made
+
+    def twin_all(batch, count):
+        ref = PR.at[pl.ds(0, count)]
+        return pltpu.make_async_remote_copy(
+            src_ref=ref, dst_ref=ref, send_sem=tw_ss, recv_sem=tw_rs.at[batch],
+            device_id=twin, device_id_type=MESH,
+        )
+
+    def pass_on(batch, made):
+        twin_all(batch, len(made)).wait_recv()
+        for at in made:
+            Pb[at] = (PP[core, at] + PR[at]).astype(BF16)
+            R[chip, at] = Pb[at, chip]
+        for at in made:
+            for j in range(1, CHIPS):
+                to = lax.rem(chip + j, CHIPS)
+                pltpu.make_async_remote_copy(
+                    src_ref=Pb.at[at, to], dst_ref=R.at[chip, at], send_sem=rs_ss,
+                    recv_sem=rs_rs.at[batch], device_id=(sp, 2 * to + core), device_id_type=MESH,
+                ).start()
+
+    def owned_all(batch, count):
+        ref = R.at[pl.ds(0, CHIPS - 1), pl.ds(0, count)]
+        return pltpu.make_async_remote_copy(
+            src_ref=ref, dst_ref=ref, send_sem=rs_ss, recv_sem=rs_rs.at[batch],
+            device_id=twin, device_id_type=MESH,
+        )
+
+    def add_up(batch, made):
+        owned_all(batch, len(made)).wait_recv()
+        for at in made:
+            total = R[0, at].astype(F32)
+            for j in range(1, CHIPS):
+                total = total + R[j, at].astype(F32)
+            T[at] = total
+
+    made0 = make(0, at_hop(0) + at_hop(1))
+    wout.forward(4, 0, 4)
+    made1 = make(1, at_hop(2))
+    wout.forward(4, 4, 8)
+    pass_on(0, made0)
+    made2 = make(2, at_hop(3))
+    pass_on(1, made1)
+    pass_on(2, made2)
     wout.last()
-    chunks([(0, ring(y, 4)), (1, ring(z, 4))])
-
+    made3 = make(3, at_hop(4))
+    pass_on(3, made3)
+    add_up(0, made0)
+    add_up(1, made1)
+    add_up(2, made2)
+
+    twin_all(0, 2 * RING).wait_send()
     kv_copy.wait_send()
     carry_all(CY, cy_ss, cy_rs).wait_send()
     carry_all(CZ, cz_ss, cz_rs).wait_send()
     win.drain()
     wout.drain()
-    whole = pltpu.make_async_remote_copy(
-        src_ref=R.at[pl.ds(0, 7)], dst_ref=R.at[pl.ds(0, 7)], send_sem=rs_ss, recv_sem=rs_rs,
-        device_id=peers[0], device_id_type=MESH,
-    )
-    whole.wait_send()
-    whole.wait_recv()
-
-    square = jnp.zeros((16, 1), F32)
-    sums = []
-    for at in range(2 * RING):
-        total = R[0, at].astype(F32)
-        for j in range(1, TP):
-            total = total + R[j, at].astype(F32)
-        sums.append(total)
-        square = square + jnp.sum(total * total, axis=-1, keepdims=True)
+    owned_all(0, 2 * RING).wait_send()
+    add_up(3, made3)
+
+    def total_square():
+        square = jnp.zeros((16, 256), F32)
+        for at in range(2 * RING):
+            square = square + T[at] * T[at]
+        return jnp.sum(square, axis=-1, keepdims=True)
+
+    square = total_square()
     scale = lax.rsqrt(square * (1.0 / D) + EPS)
     quarter = iota((16, 128), 1) // 32
     for n in range(32):
         zz, y0 = n // 4, 2 * (n % 4)
         tile = None
-        pieces = ((sums[y0], zz), (sums[RING + zz], y0), (sums[y0 + 1], zz), (sums[RING + zz], y0 + 1))
+        pieces = ((y0, zz), (RING + zz, y0), (y0 + 1, zz), (RING + zz, y0 + 1))
         for place, (source, at) in enumerate(pieces):
-            part = source[:, 128 * (at // 4) : 128 * (at // 4) + 128]
+            part = T[source, :, 128 * (at // 4) : 128 * (at // 4) + 128]
             shift = (32 * place - 32 * (at % 4)) % 128
             if shift:
                 part = pltpu.roll(part, shift, 1)
@@ -537,19 +621,21 @@
     vm, dma = pltpu.VMEM, pltpu.SemaphoreType.DMA
     spec = pl.BlockSpec(memory_space=pl.ANY)
     specs = [spec] * 18
-    specs[6] = specs[9] = pl.BlockSpec(memory_space=pltpu.SMEM)
     return pl.pallas_call(
         kernel,
         out_shape=jax.ShapeDtypeStruct((16, D), BF16),
         in_specs=specs,
         out_specs=pl.BlockSpec(memory_space=pltpu.VMEM),
         scratch_shapes=[
-            vm((64, 64, NIN), BF16),
-            vm((64, 64, 512), BF16),
+            vm((2, 64, 32, NIN), BF16),
+            vm((2, 64, 32, 512), BF16),
             vm((ROWS, D), BF16),
             vm((ROWS, D), BF16),
+            vm((2, RING, ROWS, 256), BF16),
             vm((64, 64), BF16),
             vm((64, 64), BF16),
+            pltpu.SMEM((4,), F32),
+            pltpu.SMEM((16,), F32),
             vm((1, D), F32),
             vm((1, D), F32),
             vm((1, 256), F32),
@@ -577,12 +663,15 @@
             vm((2, ROWS, 128), BF16),
             vm((ROWS, 256), BF16),
             vm((ROWS, 512), BF16),
-            vm((2 * RING, TP, 16, 256), BF16),
-            vm((TP, 2 * RING, 16, 256), BF16),
-            dma((16,)),
+            vm((2, 2 * RING, CHIPS, 16, 256), F32),
+            vm((2 * RING, CHIPS, 16, 256), F32),
+            vm((2 * RING, CHIPS, 16, 256), BF16),
+            vm((CHIPS, 2 * RING, 16, 256), BF16),
+            vm((2 * RING, 16, 256), F32),
+            dma((22,)),
             dma, dma((2, 2, 4)), dma((2, 2, 4, RING)),
             dma, dma((2, 2, 4)), dma((2, 2, 4, RING)),
-            dma, dma, dma, dma, dma, dma, dma, dma,
+            dma, dma, dma, dma, dma, dma, dma, dma((4,)), dma, dma((4,)),
         ],
         compiler_params=pltpu.CompilerParams(collective_id=0, has_side_effects=True),
     )(

time: 87.6 us -> 84.7 us (0.967)
  Pallas kernels: 85.9 us -> 82.9 us
    pallas_call x1, Pallas kernels: 85.9 us -> 82.9 us  [body(): pl.pallas_call(kernel, out_shape=jax.ShapeDtypeStruct((16, D), BF16), in_...]
where the time goes in v2:
time: 84.7 us; the launch traced here: 84.5 us
  Pallas kernels  82.9 us (98%)
  local copies, waits for them, and re-layouts  1.57 us (2%)
    pallas_call x1, Pallas kernels, body(): pl.pallas_call(kernel, out_shape=jax.ShapeDtypeStruct((16, D), BF16), in_...  82.9 us

profile of v2, /device:TPU:1, one launch (start us, length us, event | category | flops | bytes accessed | tf_op | source)
XLA Modules:
  0.0 84.5 jit_solution(9846576997272382712)
XLA Ops:
  0.0 82.9 %shard_map.172 = bf16[16,4096]{1,0:T(8,128)(2,1)} custom-call(bf16[128,4096]{1,0:T(8,128)(2,1)} %tok_h.1, f32[1,4096]{1,0:T(1,128)} %bitcast.11, bf16[64,256]{1,0:T(8,128)(2,1)} %wq_h.1, bf16[64,64]{1,0:T(8,128)(2,1)} %wk_h.1, bf16[64,64]{1,0:T(8,128)(2,1)} %wv_h.1, bf16[64,256]{1,0:T(8,128)(2,1)} %ws_h.1, f32[4]{0:T(128)} %sink_h.1, f32[16,64]{1,0:T(8,128)} %dec_h.1, ...), custom_call_target="tpu_custom_call" | custom-call | tf_op jit(solution)/shard_map/pallas_call | solution.py:624
  82.9 1.6 %copy.20 = bf16[16,4096]{1,0:T(8,128)(2,1)} copy(bf16[16,4096]{1,0:T(8,128)(2,1)} %shard_map.172) | data formatting | bytes 262144

commit v3 on v2

v3 whole, which is shorter than its diff:
```python
import math

import jax
import jax.numpy as jnp
from jax import lax
from jax.experimental import pallas as pl
from jax.experimental.pallas import tpu as pltpu
from jax.sharding import PartitionSpec as P

MESH = pl.DeviceIdType.MESH
F32 = jnp.float32
BF16 = jnp.bfloat16
EPS = 1e-06
BASE = 500000.0
RING = 8
TP = 8
CHIPS = 4
ROWS = 128
D = 4096
NQ = 384
NST = 1024
GROUPS = ((0,), (1, 2), (3, 4), (5, 6), (7,))
FLOWS = tuple((half, side) for half in (0, 1) for side in (0, 1))


ORDER = (
    ("stage", "S", 1),
    ("forward", "S", 2, 0),
    ("forward", "Q", 2, 0),
    ("stage", "Q", 1),
    ("stage", "S", 2),
    ("forward", "S", 2, 1),
    ("forward", "Q", 3, 0),
    ("stage", "Q", 2),
    ("stage", "S", 3),
    ("forward", "S", 3, 0),
    ("forward", "S", 2, 2),
    ("forward", "S", 3, 1),
    ("forward", "Q", 2, 1),
    ("norm",),
    ("stage", "S", 4),
    ("stage", "Q", 3),
    ("forward", "S", 2, 3),
    ("stage", "O", 1),
    ("forward", "S", 2, 4),
    ("stage", "Q", 4),
    ("forward", "S", 3, 2),
    ("forward", "Q", 2, 2),
    ("forward", "S", 4, 0),
    ("halves",),
    ("project", "S", 0),
    ("tables",),
    ("forward", "Q", 2, 3),
    ("forward", "S", 3, 3),
    ("project", "Q", 0),
    ("forward", "S", 3, 4),
    ("params",),
    ("forward", "Q", 2, 4),
    ("in",),
    ("forward", "Q", 3, 1),
    ("forward", "S", 4, 1),
    ("forward", "S", 4, 2),
    ("forward", "Q", 3, 2),
    ("forward", "S", 4, 3),
    ("forward", "S", 4, 4),
    ("forward", "Q", 3, 3),
    ("stage", "O", 2),
    ("forward", "Q", 3, 4),
    ("project", "Q", 1),
    ("forward", "Q", 4, 0),
    ("project", "S", 1),
    ("project", "S", 2),
    ("project", "S", 3),
    ("project", "S", 4),
    ("forward", "Q", 4, 1),
    ("forward", "Q", 4, 2),
    ("scan",),
    ("forward", "Q", 4, 3),
    ("stage", "O", 3),
    ("forward", "Q", 4, 4),
    ("forward", "O", 2, 0),
    ("forward", "O", 2, 1),
    ("stage", "O", 4),
    ("forward", "O", 2, 2),
    ("project", "Q", 2),
    ("project", "Q", 3),
    ("row",),
    ("project", "Q", 4),
    ("keys",),
    ("forward", "O", 2, 3),
    ("forward", "O", 3, 0),
    ("out",),
    ("forward", "O", 2, 4),
    ("forward", "O", 3, 1),
    ("forward", "O", 3, 2),
    ("attention",),
    ("forward", "O", 3, 3),
    ("column",),
    ("forward", "O", 3, 4),
    ("make", 0),
    ("forward", "O", 4, 0),
    ("forward", "O", 4, 1),
    ("make", 1),
    ("forward", "O", 4, 2),
    ("pass_on", 0),
    ("forward", "O", 4, 3),
    ("forward", "O", 4, 4),
    ("make", 2),
    ("pass_on", 1),
    ("pass_on", 2),
)


def nn(a, b):
    return lax.dot_general(a, b, (((1,), (0,)), ((), ())), preferred_element_type=F32)


def nt(a, b):
    return lax.dot_general(a, b, (((1,), (1,)), ((), ())), preferred_element_type=F32)


def split(x):
    high = x.astype(BF16)
    return high, (x - high.astype(F32)).astype(BF16)


def iota(shape, dim):
    return lax.broadcasted_iota(jnp.int32, shape, dim)


def ring(v, d):
    return lax.rem(v + d + 2 * RING, RING)


def cmul(ar, ai, br, bi):
    return ar * br - ai * bi, ar * bi + ai * br


def kernel(
    tok_h, ng_h, wq_h, wk_h, wv_h, ws_h, sink_h, dec_h, rot_h, ls_h,
    inre_h, inim_h, outre_h, outim_h, sg_h, wa_h, wso_h, og_h,
    out_ref,
    Ws, Wq, Wo, tok, xn, xh, kw, vw, sink_s, ls_s, ng, og, sg, dec, rot, inre, inim, outre, outim,
    us, qkv, cosr, sinr, prow, pw, BDi, BDo, Sr, Si, Er, Ei, Cr, Ci, CY, CZ, KVb, qb, M, PP, PR, Pb, R, Pl, Rl, T, upr,
    lsem, s_ssem, s_r1, s_r2, q_ssem, q_r1, q_r2, o_ssem, o_r1, o_r2, kv_ss, kv_rs, cy_ss, cy_rs, cz_ss, cz_rs,
    rs_ss, rs_rs, tw_ss, tw_rs, last_ss, last_rs,
):
    sp = lax.axis_index("sp")
    t = lax.axis_index("tp")
    z = sp // RING
    y = lax.rem(sp, RING)

    chip = t // 2
    core = lax.rem(t, 2)
    twin = (sp, t + 1 - 2 * core)
    barrier = pltpu.get_barrier_semaphore()
    after = lax.rem(sp + 1, RING * RING)
    before = lax.rem(sp + RING * RING - 1, RING * RING)
    peers = [(z * RING + ring(y, j), t) for j in range(1, RING)]
    peers += [(ring(z, j) * RING + y, t) for j in range(1, RING)]
    peers += [(sp, lax.rem(t + j, TP)) for j in range(1, TP)]
    peers += [(after, t), (before, t)]
    for peer in peers:
        pl.semaphore_signal(barrier, inc=1, device_id=peer, device_id_type=MESH)

    mine = (y * RING + z, z * RING + y)
    local = []
    for half in (0, 1):
        at = pl.ds(32 * half, 32)
        local += [
            (wq_h.at[at], Wq.at[half, mine[half], :, pl.ds(0, 256)]),
            (ws_h.at[at], Ws.at[half, mine[half]]),
        ]
    local += [
        (wk_h, kw),
        (wv_h, vw),
        (tok_h, tok),
        (ng_h, ng),
        (dec_h, dec),
        (rot_h, rot),
        (inre_h, inre),
        (inim_h, inim),
        (outre_h, outre),
        (outim_h, outim),
        (sg_h, sg),
        (og_h, og),
        (sink_h, sink_s),
        (ls_h, ls_s),
    ]
    for half in (0, 1):
        at = pl.ds(32 * half, 32)
        local += [
            (wa_h.at[at], Wo.at[half, mine[half], :, pl.ds(0, 256)]),
            (wso_h.at[at], Wo.at[half, mine[half], :, pl.ds(256, 256)]),
        ]
    copies = [pltpu.make_async_copy(a, b, lsem.at[i]) for i, (a, b) in enumerate(local)]
    for c in copies:
        c.start()

    for i in range(6):
        copies[i].wait()
    lane64 = iota((64, 128), 1)
    row64 = iota((64, 128), 0)
    to_low = (lane64 == row64).astype(F32).astype(BF16)
    to_high = (lane64 == row64 + 64).astype(F32).astype(BF16)
    kv_part = (nn(kw[...], to_low) + nn(vw[...], to_high)).astype(BF16)
    Wq[0, mine[0], :, 256:384] = kv_part[:32]
    Wq[1, mine[1], :, 256:384] = kv_part[32:]
    pl.semaphore_wait(barrier, len(peers))

    def block(half, d1, d2):
        first, second = (z, y) if half == 0 else (y, z)
        return ring(second, d2) * RING + ring(first, d1)

    def neighbour(half, phase, side):
        step = 1 if side == 0 else -1
        if (half == 0) == (phase == 1):
            return (ring(z, step) * RING + y, t)
        return (z * RING + ring(y, step), t)

    def rows(hop, side):
        return pl.ds(0, 32) if hop < 4 else pl.ds(16 * side, 16)

    def piece(buf, ssem, rsem, half, phase, hop, side, index):
        ref = buf.at[half, index, rows(hop, side)]
        return pltpu.make_async_remote_copy(
            src_ref=ref, dst_ref=ref, send_sem=ssem, recv_sem=rsem,
            device_id=neighbour(half, phase, side), device_id_type=MESH,
        )

    def sign(side):
        return 1 if side == 0 else -1

    def offset(k):
        if isinstance(k, int):
            return k // 2 if k % 2 == 0 else -((k + 1) // 2)
        return (1 - 2 * lax.rem(k, 2)) * ((k + 1) // 2)

    class Gather:
        def __init__(self, buf, ssem, r1, r2):
            self.buf, self.ssem, self.r1, self.r2 = buf, ssem, r1, r2

        def first(self, half, side, hop):
            index = block(half, -(hop - 1) * sign(side), 0)
            return piece(self.buf, self.ssem, self.r1.at[hop - 1], half, 1, hop, side, index)

        def second(self, half, side, hop, k):
            group = 15 if hop == 4 else 5 * (hop - 1) + (k + 1) // 2
            index = block(half, offset(k), -(hop - 1) * sign(side))
            return piece(self.buf, self.ssem, self.r2.at[group], half, 2, hop, side, index)

        def arrived(self, sem, count, hop):
            ref = self.buf.at[:, pl.ds(0, 2 * count), rows(hop, 0)]
            pltpu.make_async_remote_copy(
                src_ref=ref, dst_ref=ref, send_sem=self.ssem, recv_sem=sem,
                device_id=neighbour(0, 1, 0), device_id_type=MESH,
            ).wait_recv()

        def begin(self):
            for half, side in FLOWS:
                self.first(half, side, 1).start()

        def own(self, k):
            for half, side in FLOWS:
                self.second(half, side, 1, k).start()

        def stage(self, hop):
            self.arrived(self.r1.at[hop - 1], 1, hop)
            if hop < 4:
                for half, side in FLOWS:
                    self.first(half, side, hop + 1).start()
            self.own(2 * hop - 1)
            if hop < 4:
                self.own(2 * hop)

        def forward(self, hop, group):
            pieces = GROUPS[group]
            self.arrived(self.r2.at[5 * (hop - 2) + group], len(pieces), hop - 1)
            for half, side in FLOWS:
                for k in pieces:
                    self.second(half, side, hop, k).start()

        def last(self):
            self.arrived(self.r2.at[15], RING, 4)

        def drain(self):
            ref = self.buf.at[:, pl.ds(0, 63)]
            pltpu.make_async_remote_copy(
                src_ref=ref, dst_ref=ref, send_sem=self.ssem, recv_sem=self.r1.at[0],
                device_id=neighbour(0, 1, 0), device_id_type=MESH,
            ).wait_send()

    wst = Gather(Ws, s_ssem, s_r1, s_r2)
    wqk = Gather(Wq, q_ssem, q_r1, q_r2)
    wout = Gather(Wo, o_ssem, o_r1, o_r2)

    for i in (18, 19, 20, 21):
        copies[i].wait()
    for gather in (wst, wqk, wout):
        gather.begin()
        gather.own(0)

    lane_full = iota((ROWS, 128), 1)
    low_half = lax.rem(lane_full, 64) < 32
    spread64 = (lax.rem(iota((64, NST), 1), 64) == iota((64, NST), 0)).astype(F32)
    permute = (
        iota((ROWS, ROWS), 1)
        == 16 * lax.rem(iota((ROWS, ROWS), 0), 8) + iota((ROWS, ROWS), 0) // 8
    ).astype(F32).astype(BF16)
    def carry_copy(buf, ss, rs, at, peer):
        return pltpu.make_async_remote_copy(
            src_ref=buf.at[at], dst_ref=buf.at[at], send_sem=ss, recv_sem=rs,
            device_id=peer, device_id_type=MESH,
        )

    def carry_all(buf, ss, rs):
        return carry_copy(buf, ss, rs, pl.ds(0, 7), peers[0])

    kv_copy = pltpu.make_async_remote_copy(
        src_ref=KVb.at[1], dst_ref=KVb.at[0], send_sem=kv_ss, recv_sem=kv_rs,
        device_id=(after, t), device_id_type=MESH,
    )
    def swapped(x):
        return jnp.where(low_half, pltpu.roll(x, 96, 1), pltpu.roll(x, 32, 1))

    spread64b = spread64.astype(BF16)
    own_block = iota((256, NST), 0) // 16 == iota((256, NST), 1) // 64

    def diagonal(dst, at, value):
        for part, value in enumerate(split(value.reshape(256, 64))):
            dst[at + part] = jnp.where(own_block, nn(value, spread64b), 0.0).astype(BF16)

    def norm():
        copies[6].wait()
        copies[7].wait()

        def norm_step(i, c):
            at = pl.ds(pl.multiple_of(i * 16, 16), 16)
            x = tok[at, :].astype(F32)
            scale = lax.rsqrt(jnp.mean(x * x, axis=-1, keepdims=True) + EPS)
            xn[at, :] = (x * scale * ng[...]).astype(BF16)
            return c

        lax.fori_loop(0, ROWS // 16, norm_step, 0)

    def halves():
        lane128 = iota((ROWS, 128), 1) // 32
        source = iota((512, 256), 0)
        target = iota((512, 256), 1)
        spot = 64 * (target // 32) + lax.rem(target, 32)
        picks = [(source == spot + 32 * half).astype(F32).astype(BF16) for half in (0, 1)]
        for i in range(RING):
            xh[1, i] = nn(xn[:, 512 * i : 512 * i + 512], picks[1]).astype(BF16)
        for group in range(2):
            rolled = []
            for i in range(4):
                at = 512 * (4 * group + i)
                part = nn(xn[:, at : at + 512], picks[0])
                rolled.append((part[:, :128], part[:, 128:]))
            for j in range(RING):
                tile = None
                for i in range(4):
                    part = rolled[i][j // 4]
                    shift = 32 * ((i - j) % 4)
                    if shift:
                        part = pltpu.roll(part, shift, 1)
                    tile = part if tile is None else jnp.where(lane128 == i, part, tile)
                xh[0, j, :, 128 * group : 128 * group + 128] = tile.astype(BF16)


    def tables():
        lane = iota((1, 128), 1)
        freq = jnp.zeros((1, 128), F32)
        for i in range(32):
            freq = jnp.where(lax.rem(lane, 32) == i, F32(BASE ** (-2.0 * i / 64)), freq)
        position = (sp * ROWS + iota((ROWS, 128), 0)).astype(F32)
        angle = position * freq
        cosr[...] = jnp.cos(angle)
        sine = jnp.sin(angle)
        sinr[...] = jnp.where(low_half, -sine, sine)

    def params():
        for i in (8, 9, 17):
            copies[i].wait()
        lane_n = iota((1, NST), 1)
        own_group = iota((16, NST), 1) // 64 == iota((16, NST), 0)

        def as_row(ref):
            tiled = lax.dot_general(
                ref[...], spread64, (((1,), (0,)), ((), ())),
                precision=lax.Precision.HIGHEST, preferred_element_type=F32,
            )
            return jnp.sum(jnp.where(own_group, tiled, 0.0), axis=0, keepdims=True)

        lam_re = -as_row(dec)
        lam_im = as_row(rot)
        step_log = jnp.zeros((1, NST), F32)
        for g in range(16):
            step_log = jnp.where(lane_n // 64 == g, ls_s[g], step_log)
        delta = jnp.exp(step_log)
        modulus = jnp.exp(lam_re * delta)
        pr = modulus * jnp.cos(lam_im * delta)
        pi = modulus * jnp.sin(lam_im * delta)
        less = pr - 1.0
        den = lam_re * lam_re + lam_im * lam_im
        prow[0:1, :] = (less * lam_re + pi * lam_im) / den
        prow[1:2, :] = (pi * lam_re - less * lam_im) / den
        ar, ai = pr, pi
        for k in range(16):
            pw[0, k : k + 1, :] = ar
            pw[1, k : k + 1, :] = ai
            if k < 15:
                ar, ai = cmul(ar, ai, pr, pi)
        prow[2:3, :] = ar
        prow[3:4, :] = ai
        for _ in range(3):
            ar, ai = cmul(ar, ai, ar, ai)
        prow[4:5, :] = ar
        prow[5:6, :] = ai
        for _ in range(3):
            ar, ai = cmul(ar, ai, ar, ai)
        prow[6:7, :] = ar
        prow[7:8, :] = ai

    def diag_in():
        for i in (10, 11, 12, 13):
            copies[i].wait()
        diagonal(BDi, 0, inre[...])
        diagonal(BDi, 2, inim[...])

    def diag_out():
        diagonal(BDo, 0, outre[...])
        diagonal(BDo, 2, -outim[...])
        for i in (14, 15, 16):
            copies[i].wait()

    def at_hop(hop):
        if hop == 0:
            return [(0, y), (1, z)]
        if hop == 4:
            return [(0, ring(y, 4)), (1, ring(z, 4))]
        return [(0, ring(y, hop)), (0, ring(y, -hop)), (1, ring(z, hop)), (1, ring(z, -hop))]

    def projects(weights, out, hop):
        for n, (half, a) in enumerate(at_hop(hop)):
            wide = weights[half, pl.ds(pl.multiple_of(a * RING, RING), RING)]
            part = nn(xh[half, a], wide.reshape(256, out.shape[1]))
            out[...] = part if hop == 0 and n == 0 else out[...] + part

    def scan():
        u = us[...].astype(BF16)
        up = nn(permute, u).astype(BF16)
        upr[...] = up
        Sr[...] = nn(up, BDi[0]) + nn(up, BDi[1])
        Si[...] = nn(up, BDi[2]) + nn(up, BDi[3])
        fr, fi = prow[0:1, :], prow[1:2, :]
        pr, pi = pw[0, 0:1, :], pw[1, 0:1, :]
        sr = jnp.zeros((8, NST), F32)
        si = jnp.zeros((8, NST), F32)
        for i in range(16):
            at = slice(8 * i, 8 * i + 8)
            br, bi = cmul(fr, fi, Sr[at, :], Si[at, :])
            sr, si = cmul(pr, pi, sr, si)
            sr, si = sr + br, si + bi
            Sr[at, :] = sr
            Si[at, :] = si
        Er[...] = sr
        Ei[...] = si
        qr, qi = prow[2:3, :], prow[3:4, :]
        cr = jnp.zeros((1, NST), F32)
        ci = jnp.zeros((1, NST), F32)
        for j in range(8):
            cr, ci = cmul(qr, qi, cr, ci)
            cr, ci = cr + Er[j : j + 1, :], ci + Ei[j : j + 1, :]
        CY[y, 0:1, :] = cr
        CY[y, 1:2, :] = ci

        for j in range(1, RING):
            carry_copy(CY, cy_ss, cy_rs, y, (z * RING + ring(y, j), t)).start()

    def carry_row():
        carry_all(CY, cy_ss, cy_rs).wait_recv()
        br, bi = prow[4:5, :], prow[5:6, :]
        cr = jnp.zeros((1, NST), F32)
        ci = jnp.zeros((1, NST), F32)
        rowr, rowi = cr, ci
        wr, wi = cr + 1.0, ci
        for j in range(RING):
            keep = jnp.where(y == j, 1.0, 0.0).astype(F32)
            rowr = rowr + keep * cr
            rowi = rowi + keep * ci
            cr, ci = cmul(br, bi, cr, ci)
            cr, ci = cr + CY[j, 0:1, :], ci + CY[j, 1:2, :]
            go = jnp.where(y > j, 1.0, 0.0).astype(F32)
            nr, ni = cmul(br, bi, wr, wi)
            wr = wr + go * (nr - wr)
            wi = wi + go * (ni - wi)
        CZ[z, 0:1, :] = cr
        CZ[z, 1:2, :] = ci
        Cr[0:1, :] = rowr
        Ci[0:1, :] = rowi
        Cr[1:2, :] = wr
        Ci[1:2, :] = wi
        for j in range(1, RING):
            carry_copy(CZ, cz_ss, cz_rs, z, (ring(z, j) * RING + y, t)).start()


    def carry_column():
        qr, qi = prow[2:3, :], prow[3:4, :]
        carry_all(CZ, cz_ss, cz_rs).wait_recv()
        br, bi = prow[6:7, :], prow[7:8, :]
        cr = jnp.zeros((1, NST), F32)
        ci = jnp.zeros((1, NST), F32)
        for j in range(RING - 1):
            go = jnp.where(z > j, 1.0, 0.0).astype(F32)
            nr, ni = cmul(br, bi, cr, ci)
            nr, ni = nr + CZ[j, 0:1, :], ni + CZ[j, 1:2, :]
            cr = go * nr + (1.0 - go) * cr
            ci = go * ni + (1.0 - go) * ci
        cr, ci = cmul(Cr[1:2, :], Ci[1:2, :], cr, ci)
        cr, ci = cr + Cr[0:1, :], ci + Ci[0:1, :]
        for j in range(8):
            Cr[j : j + 1, :] = cr
            Ci[j : j + 1, :] = ci
            cr, ci = cmul(qr, qi, cr, ci)
            cr, ci = cr + Er[j : j + 1, :], ci + Ei[j : j + 1, :]
        cr, ci = Cr[...], Ci[...]
        for i in range(16):
            at = slice(8 * i, 8 * i + 8)
            gr, gi = cmul(pw[0, i : i + 1, :], pw[1, i : i + 1, :], cr, ci)
            Sr[at, :] = Sr[at, :] + gr
            Si[at, :] = Si[at, :] + gi
        total = upr[...].astype(F32) * sg[...]
        for j, ref in ((0, Sr), (2, Si)):
            high, low = split(ref[...])
            total = total + nt(high, BDo[j]) + nt(low, BDo[j])
        mixed = jax.nn.gelu(total).astype(BF16)
        M[:, 256:512] = lax.dot_general(
            permute, mixed, (((0,), (0,)), ((), ())), preferred_element_type=F32
        ).astype(BF16)


    def keys():
        kv = qkv[:, 256:384]
        key_lane = lane_full < 64
        kv = kv * jnp.where(key_lane, cosr[...], 1.0) + swapped(kv) * jnp.where(
            key_lane, sinr[...], 0.0
        )
        KVb[1] = kv.astype(BF16)
        kv_copy.start()

        for pair in range(2):
            x = qkv[:, 128 * pair : 128 * pair + 128]
            qb[:, 128 * pair : 128 * pair + 128] = (x * cosr[...] + swapped(x) * sinr[...]).astype(BF16)

    def attention():
        kv_copy.wait_recv()
        both = KVb[...].reshape(2 * ROWS, 128).astype(F32)
        turned = pltpu.roll(both, 64, 1)
        first_half = iota((2 * ROWS, 128), 1) < 64
        k_low = jnp.where(first_half, both, 0.0).astype(BF16)
        k_high = jnp.where(first_half, 0.0, turned).astype(BF16)
        v_low = jnp.where(first_half, turned, 0.0).astype(BF16)
        v_high = jnp.where(first_half, 0.0, both).astype(BF16)
        gap = iota((ROWS, 2 * ROWS), 0) + ROWS - iota((ROWS, 2 * ROWS), 1)
        key_at = sp * ROWS - ROWS + iota((ROWS, 2 * ROWS), 1)
        visible = (gap >= 0) & (gap < ROWS) & (key_at >= 0)

        def attend(pair):
            q = qb[:, 128 * pair : 128 * pair + 128]
            total = None
            for side, (k, v) in enumerate(((k_low, v_low), (k_high, v_high))):
                score = jnp.where(visible, nt(q, k) * 0.125, -jnp.inf)
                sink = sink_s[2 * pair + side]
                top = jnp.maximum(jnp.max(score, axis=-1, keepdims=True), sink)
                e = jnp.exp(score - top)
                weight = e / (jnp.sum(e, axis=-1, keepdims=True) + jnp.exp(sink - top))
                part = nn(weight.astype(BF16), v)
                total = part if total is None else total + part
            M[:, 128 * pair : 128 * pair + 128] = total.astype(BF16)


        attend(0)
        attend(1)

    def chunk(half, a, slot=None):
        wide = Wo[half, pl.ds(pl.multiple_of(a * RING, RING), RING)].reshape(256, 512)
        part = nt(M[...], wide)
        at = a + RING * half
        if slot is not None:
            Pl[slot] = part.astype(BF16).reshape(TP, 16, 256)
            Rl[t, slot] = Pl[slot, t]
            return at
        part = part.reshape(CHIPS, 2, 16, 256)
        PP[0, at] = part[:, 0]
        PP[1, at] = part[:, 1]
        return at

    def make(batch, items):
        made = [chunk(half, a) for half, a in items]
        for at in made:
            pltpu.make_async_remote_copy(
                src_ref=PP.at[1 - core, at], dst_ref=PR.at[at], send_sem=tw_ss,
                recv_sem=tw_rs.at[batch], device_id=twin, device_id_type=MESH,
            ).start()
        return made

    def twin_all(batch, count):
        ref = PR.at[pl.ds(0, count)]
        return pltpu.make_async_remote_copy(
            src_ref=ref, dst_ref=ref, send_sem=tw_ss, recv_sem=tw_rs.at[batch],
            device_id=twin, device_id_type=MESH,
        )

    def pass_on(batch, made):
        twin_all(batch, len(made)).wait_recv()
        for at in made:
            Pb[at] = (PP[core, at] + PR[at]).astype(BF16)
            R[chip, at] = Pb[at, chip]
        for at in made:
            for j in range(1, CHIPS):
                to = lax.rem(chip + j, CHIPS)
                pltpu.make_async_remote_copy(
                    src_ref=Pb.at[at, to], dst_ref=R.at[chip, at], send_sem=rs_ss,
                    recv_sem=rs_rs.at[batch], device_id=(sp, 2 * to + core), device_id_type=MESH,
                ).start()

    def owned_all(batch, count):
        ref = R.at[pl.ds(0, CHIPS - 1), pl.ds(0, count)]
        return pltpu.make_async_remote_copy(
            src_ref=ref, dst_ref=ref, send_sem=rs_ss, recv_sem=rs_rs.at[batch],
            device_id=twin, device_id_type=MESH,
        )

    def add_up(batch, made):
        owned_all(batch, len(made)).wait_recv()
        for at in made:
            total = R[0, at].astype(F32)
            for j in range(1, CHIPS):
                total = total + R[j, at].astype(F32)
            T[at] = total

    def make_last():
        made = [chunk(half, a, slot) for slot, (half, a) in enumerate(at_hop(4))]
        for slot in range(2):
            for j in range(1, TP):
                to = lax.rem(t + j, TP)
                pltpu.make_async_remote_copy(
                    src_ref=Pl.at[slot, to], dst_ref=Rl.at[t, slot], send_sem=last_ss,
                    recv_sem=last_rs, device_id=(sp, to), device_id_type=MESH,
                ).start()
        return made

    def last_all():
        ref = Rl.at[pl.ds(0, TP - 1)]
        return pltpu.make_async_remote_copy(
            src_ref=ref, dst_ref=ref, send_sem=last_ss, recv_sem=last_rs,
            device_id=twin, device_id_type=MESH,
        )

    gathers = {"S": wst, "Q": wqk, "O": wout}
    outs = {"S": (Ws, us), "Q": (Wq, qkv)}
    calls = {
        "norm": norm, "halves": halves, "tables": tables, "params": params, "in": diag_in,
        "out": diag_out, "scan": scan, "row": carry_row, "column": carry_column, "keys": keys,
        "attention": attention,
    }
    made = {}
    for name, *where in ORDER:
        if name == "stage":
            gathers[where[0]].stage(where[1])
        elif name == "forward":
            gathers[where[0]].forward(where[1], where[2])
        elif name == "project":
            if where[1] == 4:
                gathers[where[0]].last()
            projects(*outs[where[0]], where[1])
        elif name == "make":
            batch = where[0]
            made[batch] = make(batch, at_hop(0) + at_hop(1) if batch == 0 else at_hop(batch + 1))
        elif name == "pass_on":
            pass_on(where[0], made[where[0]])
        else:
            calls[name]()
    wout.last()
    made3 = make_last()
    for batch in range(3):
        add_up(batch, made[batch])

    twin_all(0, 14).wait_send()
    kv_copy.wait_send()
    carry_all(CY, cy_ss, cy_rs).wait_send()
    carry_all(CZ, cz_ss, cz_rs).wait_send()
    wst.drain()
    wqk.drain()
    wout.drain()
    owned_all(0, 14).wait_send()
    last_all().wait_send()
    last_all().wait_recv()
    for slot, at in enumerate(made3):
        total = Rl[0, slot].astype(F32)
        for j in range(1, TP):
            total = total + Rl[j, slot].astype(F32)
        T[at] = total

    def total_square():
        square = jnp.zeros((16, 256), F32)
        for at in range(2 * RING):
            square = square + T[at] * T[at]
        return jnp.sum(square, axis=-1, keepdims=True)

    square = total_square()
    scale = lax.rsqrt(square * (1.0 / D) + EPS)
    quarter = iota((16, 128), 1) // 32
    for n in range(32):
        zz, y0 = n // 4, 2 * (n % 4)
        tile = None
        pieces = ((y0, zz), (RING + zz, y0), (y0 + 1, zz), (RING + zz, y0 + 1))
        for place, (source, at) in enumerate(pieces):
            part = T[source, :, 128 * (at // 4) : 128 * (at // 4) + 128]
            shift = (32 * place - 32 * (at % 4)) % 128
            if shift:
                part = pltpu.roll(part, shift, 1)
            tile = part if tile is None else jnp.where(quarter == place, part, tile)
        cols = slice(128 * n, 128 * n + 128)
        out_ref[:, cols] = (tile * scale * og[:, cols]).astype(BF16)


def body(
    tokens, norm_gain, w_query, w_key, w_value, w_state_in, sink_logit, decay_rate, rotation,
    log_step, in_re, in_im, out_re, out_im, skip_gain, w_attn_out, w_state_out, out_gain,
):
    vm, dma = pltpu.VMEM, pltpu.SemaphoreType.DMA
    spec = pl.BlockSpec(memory_space=pl.ANY)
    specs = [spec] * 18
    return pl.pallas_call(
        kernel,
        out_shape=jax.ShapeDtypeStruct((16, D), BF16),
        in_specs=specs,
        out_specs=pl.BlockSpec(memory_space=pltpu.VMEM),
        scratch_shapes=[
            vm((2, 64, 32, 256), BF16),
            vm((2, 64, 32, NQ), BF16),
            vm((2, 64, 32, 512), BF16),
            vm((ROWS, D), BF16),
            vm((ROWS, D), BF16),
            vm((2, RING, ROWS, 256), BF16),
            vm((64, 64), BF16),
            vm((64, 64), BF16),
            pltpu.SMEM((4,), F32),
            pltpu.SMEM((16,), F32),
            vm((1, D), F32),
            vm((1, D), F32),
            vm((1, 256), F32),
            vm((16, 64), F32),
            vm((16, 64), F32),
            vm((16, 16, 64), F32),
            vm((16, 16, 64), F32),
            vm((16, 16, 64), F32),
            vm((16, 16, 64), F32),
            vm((ROWS, 256), F32),
            vm((ROWS, NQ), F32),
            vm((ROWS, 128), F32),
            vm((ROWS, 128), F32),
            vm((8, NST), F32),
            vm((2, 16, NST), F32),
            vm((4, 256, NST), BF16),
            vm((4, 256, NST), BF16),
            vm((ROWS, NST), F32),
            vm((ROWS, NST), F32),
            vm((8, NST), F32),
            vm((8, NST), F32),
            vm((8, NST), F32),
            vm((8, NST), F32),
            vm((RING, 2, NST), F32),
            vm((RING, 2, NST), F32),
            vm((2, ROWS, 128), BF16),
            vm((ROWS, 256), BF16),
            vm((ROWS, 512), BF16),
            vm((2, 2 * RING, CHIPS, 16, 256), F32),
            vm((2 * RING, CHIPS, 16, 256), F32),
            vm((2 * RING, CHIPS, 16, 256), BF16),
            vm((CHIPS, 2 * RING, 16, 256), BF16),
            vm((2, TP, 16, 256), BF16),
            vm((TP, 2, 16, 256), BF16),
            vm((2 * RING, 16, 256), F32),
            vm((ROWS, 256), BF16),
            dma((22,)),
            dma, dma((4,)), dma((16,)),
            dma, dma((4,)), dma((16,)),
            dma, dma((4,)), dma((16,)),
            dma, dma, dma, dma, dma, dma, dma, dma((3,)), dma, dma((3,)), dma, dma,
        ],
        compiler_params=pltpu.CompilerParams(collective_id=0, has_side_effects=True),
    )(
        tokens, norm_gain.reshape(1, D), w_query, w_key, w_value, w_state_in, sink_logit,
        decay_rate, rotation, log_step, in_re.transpose(0, 2, 1), in_im.transpose(0, 2, 1),
        out_re, out_im, skip_gain.reshape(1, 256), w_attn_out.T, w_state_out.T, out_gain.reshape(1, D),
    )


def solution(mesh):
    return jax.shard_map(
        body,
        mesh=mesh,
        in_specs=(
            P("sp", None),
            P(),
            P("sp", "tp"),
            P("sp", "tp"),
            P("sp", "tp"),
            P("sp", "tp"),
            P("tp"),
            P("tp", None),
            P("tp", None),
            P("tp"),
            P("tp", None, None),
            P("tp", None, None),
            P("tp", None, None),
            P("tp", None, None),
            P("tp"),
            P("tp", "sp"),
            P("tp", "sp"),
            P(),
        ),
        out_specs=P(("sp", "tp"), None),
        check_vma=False,
    )
```

time: 84.7 us -> 79.7 us (0.941)
  Pallas kernels: 82.9 us -> 77.8 us
    pallas_call x1, Pallas kernels: 82.9 us -> 77.8 us  [body(): pl.pallas_call(kernel, out_shape=jax.ShapeDtypeStruct((16, D), BF16), in_...]
where the time goes in v3:
time: 79.7 us; the launch traced here: 79.4 us
  Pallas kernels  77.8 us (98%)
  local copies, waits for them, and re-layouts  1.57 us (2%)
    pallas_call x1, Pallas kernels, body(): pl.pallas_call(kernel, out_shape=jax.ShapeDtypeStruct((16, D), BF16), in_...  77.8 us

profile of v3, /device:TPU:1, one launch (start us, length us, event | category | flops | bytes accessed | tf_op | source)
XLA Modules:
  0.0 79.4 jit_solution(14400686021796838349)
XLA Ops:
  0.0 77.8 %shard_map.172 = bf16[16,4096]{1,0:T(8,128)(2,1)} custom-call(bf16[128,4096]{1,0:T(8,128)(2,1)} %tok_h.1, f32[1,4096]{1,0:T(1,128)} %bitcast.11, bf16[64,256]{1,0:T(8,128)(2,1)} %wq_h.1, bf16[64,64]{1,0:T(8,128)(2,1)} %wk_h.1, bf16[64,64]{1,0:T(8,128)(2,1)} %wv_h.1, bf16[64,256]{1,0:T(8,128)(2,1)} %ws_h.1, f32[4]{0:T(128)} %sink_h.1, f32[16,64]{1,0:T(8,128)} %dec_h.1, ...), custom_call_target="tpu_custom_call" | custom-call | tf_op jit(solution)/shard_map/pallas_call | solution.py:736
  77.8 1.6 %copy.20 = bf16[16,4096]{1,0:T(8,128)(2,1)} copy(bf16[16,4096]{1,0:T(8,128)(2,1)} %shard_map.172) | data formatting | bytes 262144

commit v4 on v3

--- a/solution.py
+++ b/solution.py
@@ -197,7 +197,99 @@
     for c in copies:
         c.start()
 
-    for i in range(6):
+    for i in (1, 3):
+        copies[i].wait()
+    pl.semaphore_wait(barrier, len(peers))
+
+    def block(half, d1, d2):
+        first, second = (z, y) if half == 0 else (y, z)
+        return ring(second, d2) * RING + ring(first, d1)
+
+    def neighbour(half, phase, side):
+        step = 1 if side == 0 else -1
+        if (half == 0) == (phase == 1):
+            return (ring(z, step) * RING + y, t)
+        return (z * RING + ring(y, step), t)
+
+    def rows(hop, side):
+        return pl.ds(0, 32) if hop < 4 else pl.ds(16 * side, 16)
+
+    def piece(buf, ssem, rsem, half, phase, hop, side, index):
+        ref = buf.at[half, index, rows(hop, side)]
+        return pltpu.make_async_remote_copy(
+            src_ref=ref, dst_ref=ref, send_sem=ssem, recv_sem=rsem,
+            device_id=neighbour(half, phase, side), device_id_type=MESH,
+        )
+
+    def sign(side):
+        return 1 if side == 0 else -1
+
+    def offset(k):
+        if isinstance(k, int):
+            return k // 2 if k % 2 == 0 else -((k + 1) // 2)
+        return (1 - 2 * lax.rem(k, 2)) * ((k + 1) // 2)
+
+    class Gather:
+        def __init__(self, buf, ssem, r1, r2):
+            self.buf, self.ssem, self.r1, self.r2 = buf, ssem, r1, r2
+
+        def first(self, half, side, hop):
+            index = block(half, -(hop - 1) * sign(side), 0)
+            return piece(self.buf, self.ssem, self.r1.at[hop - 1], half, 1, hop, side, index)
+
+        def second(self, half, side, hop, k):
+            group = 15 if hop == 4 else 5 * (hop - 1) + (k + 1) // 2
+            index = block(half, offset(k), -(hop - 1) * sign(side))
+            return piece(self.buf, self.ssem, self.r2.at[group], half, 2, hop, side, index)
+
+        def arrived(self, sem, count, hop):
+            ref = self.buf.at[:, pl.ds(0, 2 * count), rows(hop, 0)]
+            pltpu.make_async_remote_copy(
+                src_ref=ref, dst_ref=ref, send_sem=self.ssem, recv_sem=sem,
+                device_id=neighbour(0, 1, 0), device_id_type=MESH,
+            ).wait_recv()
+
+        def begin(self):
+            for half, side in FLOWS:
+                self.first(half, side, 1).start()
+
+        def own(self, k):
+            for half, side in FLOWS:
+                self.second(half, side, 1, k).start()
+
+        def stage(self, hop):
+            self.arrived(self.r1.at[hop - 1], 1, hop)
+            if hop < 4:
+                for half, side in FLOWS:
+                    self.first(half, side, hop + 1).start()
+            self.own(2 * hop - 1)
+            if hop < 4:
+                self.own(2 * hop)
+
+        def forward(self, hop, group):
+            pieces = GROUPS[group]
+            self.arrived(self.r2.at[5 * (hop - 2) + group], len(pieces), hop - 1)
+            for half, side in FLOWS:
+                for k in pieces:
+                    self.second(half, side, hop, k).start()
+
+        def last(self):
+            self.arrived(self.r2.at[15], RING, 4)
+
+        def drain(self):
+            ref = self.buf.at[:, pl.ds(0, 63)]
+            pltpu.make_async_remote_copy(
+                src_ref=ref, dst_ref=ref, send_sem=self.ssem, recv_sem=self.r1.at[0],
+                device_id=neighbour(0, 1, 0), device_id_type=MESH,
+            ).wait_send()
+
+    wst = Gather(Ws, s_ssem, s_r1, s_r2)
+    wqk = Gather(Wq, q_ssem, q_r1, q_r2)
+    wout = Gather(Wo, o_ssem, o_r1, o_r2)
+
+    wst.begin()
+    wst.own(0)
+    for i in (0, 2, 4, 5):
         copies[i].wait()
     lane64 = iota((64, 128), 1)
     row64 = iota((64, 128), 0)
@@ -206,97 +298,9 @@
     kv_part = (nn(kw[...], to_low) + nn(vw[...], to_high)).astype(BF16)
     Wq[0, mine[0], :, 256:384] = kv_part[:32]
     Wq[1, mine[1], :, 256:384] = kv_part[32:]
-    pl.semaphore_wait(barrier, len(peers))
-
-    def block(half, d1, d2):
-        first, second = (z, y) if half == 0 else (y, z)
-        return ring(second, d2) * RING + ring(first, d1)
-
-    def neighbour(half, phase, side):
-        step = 1 if side == 0 else -1
-        if (half == 0) == (phase == 1):
-            return (ring(z, step) * RING + y, t)
-        return (z * RING + ring(y, step), t)
-
-    def rows(hop, side):
-        return pl.ds(0, 32) if hop < 4 else pl.ds(16 * side, 16)
-
-    def piece(buf, ssem, rsem, half, phase, hop, side, index):
-        ref = buf.at[half, index, rows(hop, side)]
-        return pltpu.make_async_remote_copy(
-            src_ref=ref, dst_ref=ref, send_sem=ssem, recv_sem=rsem,
-            device_id=neighbour(half, phase, side), device_id_type=MESH,
-        )
-
-    def sign(side):
-        return 1 if side == 0 else -1
-
-    def offset(k):
-        if isinstance(k, int):
-            return k // 2 if k % 2 == 0 else -((k + 1) // 2)
-        return (1 - 2 * lax.rem(k, 2)) * ((k + 1) // 2)
-
-    class Gather:
-        def __init__(self, buf, ssem, r1, r2):
-            self.buf, self.ssem, self.r1, self.r2 = buf, ssem, r1, r2
-
-        def first(self, half, side, hop):
-            index = block(half, -(hop - 1) * sign(side), 0)
-            return piece(self.buf, self.ssem, self.r1.at[hop - 1], half, 1, hop, side, index)
-
-        def second(self, half, side, hop, k):
-            group = 15 if hop == 4 else 5 * (hop - 1) + (k + 1) // 2
-            index = block(half, offset(k), -(hop - 1) * sign(side))
-            return piece(self.buf, self.ssem, self.r2.at[group], half, 2, hop, side, index)
-
-        def arrived(self, sem, count, hop):
-            ref = self.buf.at[:, pl.ds(0, 2 * count), rows(hop, 0)]
-            pltpu.make_async_remote_copy(
-                src_ref=ref, dst_ref=ref, send_sem=self.ssem, recv_sem=sem,
-                device_id=neighbour(0, 1, 0), device_id_type=MESH,
-            ).wait_recv()
-
-        def begin(self):
-            for half, side in FLOWS:
-                self.first(half, side, 1).start()
-
-        def own(self, k):
-            for half, side in FLOWS:
-                self.second(half, side, 1, k).start()
-
-        def stage(self, hop):
-            self.arrived(self.r1.at[hop - 1], 1, hop)
-            if hop < 4:
-                for half, side in FLOWS:
-                    self.first(half, side, hop + 1).start()
-            self.own(2 * hop - 1)
-            if hop < 4:
-                self.own(2 * hop)
-
-        def forward(self, hop, group):
-            pieces = GROUPS[group]
-            self.arrived(self.r2.at[5 * (hop - 2) + group], len(pieces), hop - 1)
-            for half, side in FLOWS:
-                for k in pieces:
-                    self.second(half, side, hop, k).start()
-
-        def last(self):
-            self.arrived(self.r2.at[15], RING, 4)
-
-        def drain(self):
-            ref = self.buf.at[:, pl.ds(0, 63)]
-            pltpu.make_async_remote_copy(
-                src_ref=ref, dst_ref=ref, send_sem=self.ssem, recv_sem=self.r1.at[0],
-                device_id=neighbour(0, 1, 0), device_id_type=MESH,
-            ).wait_send()
-
-    wst = Gather(Ws, s_ssem, s_r1, s_r2)
-    wqk = Gather(Wq, q_ssem, q_r1, q_r2)
-    wout = Gather(Wo, o_ssem, o_r1, o_r2)
-
     for i in (18, 19, 20, 21):
         copies[i].wait()
-    for gather in (wst, wqk, wout):
+    for gather in (wqk, wout):
         gather.begin()
         gather.own(0)
 
@@ -618,7 +622,7 @@
             Pb[at] = (PP[core, at] + PR[at]).astype(BF16)
             R[chip, at] = Pb[at, chip]
         for at in made:
-            for j in range(1, CHIPS):
+            for j in (2, 1, 3):
                 to = lax.rem(chip + j, CHIPS)
                 pltpu.make_async_remote_copy(
                     src_ref=Pb.at[at, to], dst_ref=R.at[chip, at], send_sem=rs_ss,
@@ -643,8 +647,8 @@
     def make_last():
         made = [chunk(half, a, slot) for slot, (half, a) in enumerate(at_hop(4))]
         for slot in range(2):
-            for j in range(1, TP):
-                to = lax.rem(t + j, TP)
+            for j in (4, 5, 2, 3, 6, 7, 1):
+                to = 2 * lax.rem(chip + j // 2, CHIPS) + lax.rem(core + j, 2)
                 pltpu.make_async_remote_copy(
                     src_ref=Pl.at[slot, to], dst_ref=Rl.at[t, slot], send_sem=last_ss,
                     recv_sem=last_rs, device_id=(sp, to), device_id_type=MESH,
@@ -735,7 +739,7 @@
     specs = [spec] * 18
     return pl.pallas_call(
         kernel,
-        out_shape=jax.ShapeDtypeStruct((16, D), BF16),
+        out_shape=pltpu.VMEM((16, D), BF16),
         in_specs=specs,
         out_specs=pl.BlockSpec(memory_space=pltpu.VMEM),
         scratch_shapes=[

time: 79.7 us -> 77.7 us (0.975)
  local copies, waits for them, and re-layouts: 1.57 us -> 0.66 us
  Pallas kernels: 77.8 us -> 76.9 us
    unnamed x1, local copies, waits for them, and re-layouts: 1.57 us -> 0.66 us
    pallas_call x1, Pallas kernels: 77.8 us -> 76.9 us  [body(): pl.pallas_call(kernel, out_shape=pltpu.VMEM((16, D), BF16), in_specs=spec...]
where the time goes in v4:
time: 77.7 us; the launch traced here: 77.6 us
  Pallas kernels  76.9 us (99%)
    pallas_call x1, Pallas kernels, body(): pl.pallas_call(kernel, out_shape=pltpu.VMEM((16, D), BF16), in_specs=spec...  76.9 us

profile of v4, /device:TPU:1, one launch (start us, length us, event | category | flops | bytes accessed | tf_op | source)
XLA Modules:
  0.0 77.6 jit_solution(2608553915797632752)
XLA Ops:
  0.0 76.9 %shard_map.172 = bf16[16,4096]{1,0:T(8,128)(2,1)S(1)} custom-call(bf16[128,4096]{1,0:T(8,128)(2,1)} %tok_h.1, f32[1,4096]{1,0:T(1,128)} %bitcast.11, bf16[64,256]{1,0:T(8,128)(2,1)} %wq_h.1, bf16[64,64]{1,0:T(8,128)(2,1)} %wk_h.1, bf16[64,64]{1,0:T(8,128)(2,1)} %wv_h.1, bf16[64,256]{1,0:T(8,128)(2,1)} %ws_h.1, f32[4]{0:T(128)} %sink_h.1, f32[16,64]{1,0:T(8,128)} %dec_h.1, ...), custom_call_target="tpu_custom_call" | custom-call | tf_op jit(solution)/shard_map/pallas_call | solution.py:740
  77.0 0.7 copy.20

commit v5 on v4

--- a/solution.py
+++ b/solution.py
@@ -137,10 +137,10 @@
 
 
 def kernel(
-    tok_h, ng_h, wq_h, wk_h, wv_h, ws_h, sink_h, dec_h, rot_h, ls_h,
+    tok_h, ng_h, wq_h, wk_h, wv_h, ws_h, sink_s, dec_h, rot_h, ls_s,
     inre_h, inim_h, outre_h, outim_h, sg_h, wa_h, wso_h, og_h,
     out_ref,
-    Ws, Wq, Wo, tok, xn, xh, kw, vw, sink_s, ls_s, ng, og, sg, dec, rot, inre, inim, outre, outim,
+    Ws, Wq, Wo, tok, xn, xh, kw, vw, ng, og, sg, dec, rot, inre, inim, outre, outim,
     us, qkv, cosr, sinr, prow, pw, BDi, BDo, Sr, Si, Er, Ei, Cr, Ci, CY, CZ, KVb, qb, M, PP, PR, Pb, R, Pl, Rl, T, upr,
     lsem, s_ssem, s_r1, s_r2, q_ssem, q_r1, q_r2, o_ssem, o_r1, o_r2, kv_ss, kv_rs, cy_ss, cy_rs, cz_ss, cz_rs,
     rs_ss, rs_rs, tw_ss, tw_rs, last_ss, last_rs,
@@ -184,8 +184,6 @@
         (outim_h, outim),
         (sg_h, sg),
         (og_h, og),
-        (sink_h, sink_s),
-        (ls_h, ls_s),
     ]
     for half in (0, 1):
         at = pl.ds(32 * half, 32)
@@ -298,7 +296,7 @@
     kv_part = (nn(kw[...], to_low) + nn(vw[...], to_high)).astype(BF16)
     Wq[0, mine[0], :, 256:384] = kv_part[:32]
     Wq[1, mine[1], :, 256:384] = kv_part[32:]
-    for i in (18, 19, 20, 21):
+    for i in (16, 17, 18, 19):
         copies[i].wait()
     for gather in (wqk, wout):
         gather.begin()
@@ -384,7 +382,7 @@
         sinr[...] = jnp.where(low_half, -sine, sine)
 
     def params():
-        for i in (8, 9, 17):
+        for i in (8, 9):
             copies[i].wait()
         lane_n = iota((1, NST), 1)
         own_group = iota((16, NST), 1) // 64 == iota((16, NST), 0)
@@ -435,7 +433,7 @@
     def diag_out():
         diagonal(BDo, 0, outre[...])
         diagonal(BDo, 2, -outim[...])
-        for i in (14, 15, 16):
+        for i in (14, 15):
             copies[i].wait()
 
     def at_hop(hop):
@@ -645,8 +643,9 @@
             T[at] = total
 
     def make_last():
-        made = [chunk(half, a, slot) for slot, (half, a) in enumerate(at_hop(4))]
-        for slot in range(2):
+        made = []
+        for slot, (half, a) in enumerate(at_hop(4)):
+            made.append(chunk(half, a, slot))
             for j in (4, 5, 2, 3, 6, 7, 1):
                 to = 2 * lax.rem(chip + j // 2, CHIPS) + lax.rem(core + j, 2)
                 pltpu.make_async_remote_copy(
@@ -737,6 +736,7 @@
     vm, dma = pltpu.VMEM, pltpu.SemaphoreType.DMA
     spec = pl.BlockSpec(memory_space=pl.ANY)
     specs = [spec] * 18
+    specs[6] = specs[9] = pl.BlockSpec(memory_space=pltpu.SMEM)
     return pl.pallas_call(
         kernel,
         out_shape=pltpu.VMEM((16, D), BF16),
@@ -751,8 +751,6 @@
             vm((2, RING, ROWS, 256), BF16),
             vm((64, 64), BF16),
             vm((64, 64), BF16),
-            pltpu.SMEM((4,), F32),
-            pltpu.SMEM((16,), F32),
             vm((1, D), F32),
             vm((1, D), F32),
             vm((1, 256), F32),
@@ -789,7 +787,7 @@
             vm((TP, 2, 16, 256), BF16),
             vm((2 * RING, 16, 256), F32),
             vm((ROWS, 256), BF16),
-            dma((22,)),
+            dma((20,)),
             dma, dma((4,)), dma((16,)),
             dma, dma((4,)), dma((16,)),
             dma, dma((4,)), dma((16,)),

time: 77.7 us -> 78.4 us (level)
  no operation moved by 1% of the time
where the time goes in v5:
time: 78.4 us; the launch traced here: 78.3 us
  Pallas kernels  77.6 us (99%)
    pallas_call x1, Pallas kernels, body(): pl.pallas_call(kernel, out_shape=pltpu.VMEM((16, D), BF16), in_specs=spec...  77.6 us

profile of v5, /device:TPU:1, one launch (start us, length us, event | category | flops | bytes accessed | tf_op | source)
XLA Modules:
  0.0 78.3 jit_solution(1807365017624905942)
XLA Ops:
  0.0 77.6 %shard_map.172 = bf16[16,4096]{1,0:T(8,128)(2,1)S(1)} custom-call(bf16[128,4096]{1,0:T(8,128)(2,1)} %tok_h.1, f32[1,4096]{1,0:T(1,128)} %bitcast.11, bf16[64,256]{1,0:T(8,128)(2,1)} %wq_h.1, bf16[64,64]{1,0:T(8,128)(2,1)} %wk_h.1, bf16[64,64]{1,0:T(8,128)(2,1)} %wv_h.1, bf16[64,256]{1,0:T(8,128)(2,1)} %ws_h.1, f32[4]{0:T(128)} %sink_s.1, f32[16,64]{1,0:T(8,128)} %dec_h.1, ...), custom_call_target="tpu_custom_call" | custom-call | tf_op jit(solution)/shard_map/pallas_call | solution.py:740
  77.6 0.7 copy.20
